TPU v7x, 512 devices: a whole 4x4x16 slice. The times are simulated.
512 devices in a mesh: sp: 64 (over z, y), tp: 8 (over x, core).
Axes of the slice: x: 4, y: 4, z: 16, core: 2. Of those that a mesh axis runs over, the one named last changes fastest.
Arguments:
- hidden_in: bfloat16 [16384, 2048], P('sp', 'tp'), may hold values from -6 to 6
- w_query_rec: bfloat16 [2048, 2048], P('sp', 'tp'), may hold values from -0.125 to 0.125
- w_forget: bfloat16 [2048, 2048], P('sp', 'tp'), may hold values from -0.125 to 0.125
- w_input: bfloat16 [2048, 2048], P('sp', 'tp'), may hold values from -0.125 to 0.125
- forget_gap: float32 [2048], P('tp'), may hold values from 1e-05 to 0.08
- decay_extra: float32 [16384, 16], P('sp', 'tp'), may hold values from -0.75 to 0
- rec_gain: float32 [128], replicated, may hold values from 0.1 to 1.9
- w_q_down: bfloat16 [2048, 512], P(None, 'tp'), may hold values from -0.125 to 0.125
- w_kv_down: bfloat16 [2048, 256], P(None, 'tp'), may hold values from -0.125 to 0.125
- w_key_rope: bfloat16 [2048, 32], replicated, may hold values from -0.125 to 0.125
- q_gain: float32 [512], replicated, may hold values from 1.4 to 7
- kv_gain: float32 [256], replicated, may hold values from 1.4 to 7
- w_q_nope: bfloat16 [512, 1024], P(None, 'tp'), may hold values from -0.25 to 0.25
- w_q_rope: bfloat16 [512, 512], P(None, 'tp'), may hold values from -0.25 to 0.25
- w_k_up: bfloat16 [256, 1024], P(None, 'tp'), may hold values from -0.375 to 0.375
- w_v_up: bfloat16 [256, 1024], P(None, 'tp'), may hold values from -0.375 to 0.375
- w_out_rec: bfloat16 [2048, 2048], P('tp'), may hold values from -0.109375 to 0.109375
- w_out_att: bfloat16 [1024, 2048], P('tp'), may hold values from -0.109375 to 0.109375
Outputs:
- mixed_out: bfloat16 [16384, 2048], P(('sp', 'tp'))
All inputs are finite; a program needn't handle non-finite values.
Results may differ from a plain program's by a relative error of at most 0.02.
The roundings to bfloat16 on the way count: a program that leaves them out, or rounds other values in their place, can miss the bound.
Values may be sent and summed in bfloat16 or wider, within the bound.
A program may use at most 128 MiB of HBM per device.

v0:
```python
import math

import jax
import jax.numpy as jnp
from jax import lax
from jax.sharding import PartitionSpec as P

HG_KDIM = 128
HG_VDIM = 128
HG_BLOCK = 64
NOPE = 64
ROPE = 32
MLA_V = 64


NORM_EPS = 1e-06
ROPE_BASE = 10000.0
NEG_BIG = -1e30


def side_by_side(arrays, axis, dim, along):
    widths = [a.shape[along] for a in arrays]
    both = jnp.concatenate(arrays, axis=along)
    whole = lax.all_gather(both, axis, axis=dim, tiled=True)
    return tuple(jnp.split(whole, [sum(widths[:k]) for k in range(1, len(widths))], axis=along))


def laid_out(blocks, dim):
    lengths = list(blocks.shape[1:])
    lengths[dim] *= blocks.shape[0]
    return jnp.moveaxis(blocks, 0, dim).reshape(lengths)


def sent_to_all(value, axis):
    devices = lax.axis_size(axis)
    return lax.all_to_all(
        jnp.broadcast_to(value[None], (devices, *value.shape)), axis, 0, 0, tiled=True
    )


def collect(value, axis, dim):
    return laid_out(sent_to_all(value, axis), dim)


def carried_in(part, axis, combine, identity):
    place = lax.axis_index(axis)
    gathered = jax.tree.map(lambda a: lax.all_gather(a, axis), part)
    state = jax.tree.map(lambda a, e: jnp.zeros_like(a) + jnp.asarray(e, a.dtype), part, identity)

    def one(step, state):
        return combine(
            state, jax.tree.map(lambda a: lax.dynamic_index_in_dim(a, step, 0, False), gathered)
        )

    return lax.fori_loop(0, place, one, state)


def one_gather(arrays, axis, dims):
    vector = jnp.concatenate([a.reshape(-1) for a in arrays])
    lines, at, outs = (lax.all_gather(vector, axis), 0, [])
    for a, dim in zip(arrays, dims):
        blocks = lines[:, at : at + a.size].reshape(-1, *a.shape)
        outs.append(laid_out(blocks, dim))
        at += a.size
    return tuple(outs)


def in_blocks(value, dim, devices):
    lengths = value.shape
    blocks = value.reshape(*lengths[:dim], devices, lengths[dim] // devices, *lengths[dim + 1 :])
    return jnp.moveaxis(blocks, dim, 0)


def summed_on_arrival(value, axis, dim):
    devices = lax.axis_size(axis)
    blocks = lax.all_to_all(in_blocks(value, dim, devices), axis, 0, 0, tiled=True)
    return jnp.sum(blocks.astype(jnp.float32), axis=0)


def rms_scale(values):
    return values * lax.rsqrt(jnp.mean(values * values, axis=-1, keepdims=True) + NORM_EPS)


def rotate_half(values, cosine, sine_table):
    half_width = values.shape[-1] // 2
    lower_half = values[..., :half_width]
    upper_half = values[..., half_width:]
    return jnp.concatenate(
        [
            lower_half * cosine - upper_half * sine_table,
            lower_half * sine_table + upper_half * cosine,
        ],
        axis=-1,
    )


def rotary_tables(row_count, offset, rot_width):
    positions = jnp.arange(row_count, dtype=jnp.float32) + offset
    frequency = 1.0 / ROPE_BASE ** (jnp.arange(0, rot_width, 2, dtype=jnp.float32) / rot_width)
    angles = positions[:, None] * frequency[None, :]
    return (jnp.cos(angles), jnp.sin(angles))


def block_step(rec_state, inputs):
    queries, key_in, values, log_forget = inputs
    cumulative = jnp.cumsum(log_forget, axis=1)
    log_gaps = cumulative[:, :, None, :] - cumulative[:, None, :, :]
    block_len = queries.shape[1]
    lower_mask = jnp.tril(jnp.ones((block_len, block_len), jnp.float32))
    decays = jnp.exp(jnp.minimum(log_gaps, 0.0)) * lower_mask[None, :, :, None]
    scores = jnp.einsum(
        "htsd,hsd->hts", queries[:, :, None, :] * decays, key_in, precision=lax.Precision.HIGHEST
    )
    block_out = jnp.einsum(
        "hts,hsv->htv", scores, values, precision=lax.Precision.HIGHEST
    ) + jnp.einsum(
        "htd,hdv->htv", queries * jnp.exp(cumulative), rec_state, precision=lax.Precision.HIGHEST
    )
    last_cumul = cumulative[:, -1:, :]
    rec_state = jnp.exp(last_cumul[:, 0, :])[..., None] * rec_state + jnp.einsum(
        "hsd,hsv->hdv",
        key_in * jnp.exp(last_cumul - cumulative),
        values,
        precision=lax.Precision.HIGHEST,
    )
    return (rec_state, block_out)


def score_block(q_nope, q_rope, k_nope, k_rope, values, q_start, k_start):
    score_scale = 1.0 / math.sqrt(NOPE + ROPE)
    scores = (
        jnp.einsum("qhd,khd->hqk", q_nope, k_nope, preferred_element_type=jnp.float32)
        + jnp.einsum("qhr,kr->hqk", q_rope, k_rope, preferred_element_type=jnp.float32)
    ) * score_scale
    q_pos = q_start + jnp.arange(q_nope.shape[0], dtype=jnp.int32)
    k_pos = k_start + jnp.arange(k_nope.shape[0], dtype=jnp.int32)
    allowed = k_pos[None, :] <= q_pos[:, None]
    scores = jnp.where(allowed[None], scores, NEG_BIG)
    block_peak = jnp.max(scores, axis=-1)
    weights = jnp.where(allowed[None], jnp.exp(scores - block_peak[..., None]), 0.0)
    block_total = jnp.sum(weights, axis=-1)
    weights16 = weights.astype(jnp.bfloat16)
    block_sum = jnp.einsum("hqk,khv->hqv", weights16, values, preferred_element_type=jnp.float32)
    return (block_peak, block_total, block_sum)


def merge_terms(earlier, later_part):
    top = jnp.maximum(earlier[0], later_part[0])
    old_factor = jnp.exp(earlier[0] - top)
    new_factor = jnp.exp(later_part[0] - top)
    return (
        top,
        earlier[1] * old_factor + later_part[1] * new_factor,
        earlier[2] * old_factor[..., None] + later_part[2] * new_factor[..., None],
    )


def chain_step(earlier, later_part):
    return (earlier[0] * later_part[0], later_part[0][..., None] * earlier[1] + later_part[1])


def shards(
    hidden_in,
    w_query_rec,
    w_forget,
    w_input,
    forget_gap,
    decay_extra,
    rec_gain,
    w_q_down,
    w_kv_down,
    w_key_rope,
    q_gain,
    kv_gain,
    w_q_nope,
    w_q_rope,
    w_k_up,
    w_v_up,
    w_out_rec,
    w_out_att,
):
    tok_dev = hidden_in.shape[0]
    sp_index = lax.axis_index("sp")
    full_query, full_forget, full_input = side_by_side((w_query_rec, w_forget, w_input), "sp", 0, 1)
    left_weight = jnp.concatenate([full_query, full_forget, full_input], axis=1)
    right_weight = jnp.concatenate([w_q_down, w_kv_down, w_key_rope], axis=1)
    feature_piece = collect(hidden_in, "tp", 1)
    left_sum = jnp.dot(feature_piece, left_weight, preferred_element_type=jnp.float32)
    right_sum = jnp.dot(feature_piece, right_weight, preferred_element_type=jnp.float32)
    key_cols = full_query.shape[1]
    head_count = key_cols // HG_KDIM
    left_round = left_sum.astype(jnp.bfloat16)
    rec_query = left_round[:, :key_cols].astype(jnp.float32).reshape(tok_dev, head_count, HG_KDIM)
    forget_pre = (
        left_round[:, key_cols : 2 * key_cols]
        .astype(jnp.float32)
        .reshape(tok_dev, head_count, HG_KDIM)
    )
    rec_value = (
        left_round[:, 2 * key_cols :].astype(jnp.float32).reshape(tok_dev, head_count, HG_VDIM)
    )
    gap_rows = forget_gap.reshape(head_count, HG_KDIM)
    closing = jax.nn.sigmoid(-forget_pre)
    key_in = gap_rows * closing
    log_forget = jnp.log1p(-gap_rows * closing) + decay_extra[:, :, None]
    block_count = tok_dev // HG_BLOCK

    def to_blocks(tensor):
        return tensor.reshape(block_count, HG_BLOCK, head_count, tensor.shape[-1]).transpose(
            0, 2, 1, 3
        )

    zero_state = jnp.zeros((head_count, HG_KDIM, HG_VDIM), jnp.float32)
    local_state, local_out = lax.scan(
        block_step,
        zero_state,
        (to_blocks(rec_query), to_blocks(key_in), to_blocks(rec_value), to_blocks(log_forget)),
    )
    local_out = local_out.transpose(0, 2, 1, 3).reshape(tok_dev, head_count, HG_VDIM)
    cumulative = jnp.cumsum(log_forget, axis=0)
    device_decay = jnp.exp(cumulative[-1])
    scanned = carried_in(
        (device_decay, local_state),
        "sp",
        chain_step,
        (jnp.ones_like(device_decay), jnp.zeros_like(local_state)),
    )
    into_state = scanned[1]
    rec_raw = local_out + jnp.einsum(
        "thd,hdv->thv", rec_query * jnp.exp(cumulative), into_state, precision=lax.Precision.HIGHEST
    )
    rec_out = (
        (rms_scale(rec_raw) * rec_gain).astype(jnp.bfloat16).reshape(tok_dev, head_count * HG_VDIM)
    )
    q_cols = w_q_down.shape[1]
    kv_cols = w_kv_down.shape[1]
    right_round = right_sum.astype(jnp.bfloat16)
    q_part = right_round[:, :q_cols]
    kv_part = right_round[:, q_cols : q_cols + kv_cols]
    rope_raw = right_sum[:, q_cols + kv_cols :]
    q_whole, kv_whole = one_gather((q_part, kv_part), "tp", (1, 1))
    q_normed = (rms_scale(q_whole.astype(jnp.float32)) * q_gain).astype(jnp.bfloat16)
    latent = (rms_scale(kv_whole.astype(jnp.float32)) * kv_gain).astype(jnp.bfloat16)
    q_start = sp_index * tok_dev
    cosine, sine_table = rotary_tables(tok_dev, q_start.astype(jnp.float32), ROPE)
    key_rope = rotate_half(rope_raw, cosine, sine_table).astype(jnp.bfloat16)
    att_heads = w_q_nope.shape[1] // NOPE
    q_nope = jnp.dot(q_normed, w_q_nope, preferred_element_type=jnp.float32).astype(jnp.bfloat16)
    q_nope = q_nope.reshape(tok_dev, att_heads, NOPE)
    q_rope = jnp.dot(q_normed, w_q_rope, preferred_element_type=jnp.float32).reshape(
        tok_dev, att_heads, ROPE
    )
    q_rope = rotate_half(q_rope, cosine[:, None, :], sine_table[:, None, :]).astype(jnp.bfloat16)

    def attend_heads(running, key_rows, value_rows, rope_rows, key_start):

        def compute(previous):
            partials = score_block(
                q_nope,
                q_rope,
                key_rows.reshape(-1, att_heads, NOPE),
                rope_rows,
                value_rows.reshape(-1, att_heads, MLA_V),
                q_start,
                key_start,
            )
            return merge_terms(previous, partials)

        return lax.cond(key_start <= q_start, compute, lambda previous: previous, running)

    initial_att = (
        jnp.full((att_heads, tok_dev), NEG_BIG, jnp.float32),
        jnp.zeros((att_heads, tok_dev), jnp.float32),
        jnp.zeros((att_heads, tok_dev, MLA_V), jnp.float32),
    )
    own_keys = jnp.dot(latent, w_k_up, preferred_element_type=jnp.float32).astype(jnp.bfloat16)
    own_values = jnp.dot(latent, w_v_up, preferred_element_type=jnp.float32).astype(jnp.bfloat16)
    key_piece, value_piece, rope_piece = side_by_side((own_keys, own_values, key_rope), "sp", 0, 1)

    def visit(block_index, current):
        first_row = block_index * tok_dev
        return attend_heads(
            current,
            lax.dynamic_slice_in_dim(key_piece, first_row, tok_dev, 0),
            lax.dynamic_slice_in_dim(value_piece, first_row, tok_dev, 0),
            lax.dynamic_slice_in_dim(rope_piece, first_row, tok_dev, 0),
            first_row,
        )

    top, total_w, accum = lax.fori_loop(0, key_piece.shape[0] // tok_dev, visit, initial_att)
    att_out = (accum / total_w[..., None]).transpose(1, 0, 2).reshape(tok_dev, att_heads * MLA_V)
    att_out = att_out.astype(jnp.bfloat16)
    mixed_out = summed_on_arrival(
        (
            jnp.dot(rec_out, w_out_rec, preferred_element_type=jnp.float32)
            + jnp.dot(att_out, w_out_att, preferred_element_type=jnp.float32)
        ).astype(jnp.bfloat16),
        "tp",
        0,
    )
    return mixed_out.astype(jnp.bfloat16)


def solution(mesh):
    placed = (
        P("sp", "tp"),
        P("sp", "tp"),
        P("sp", "tp"),
        P("sp", "tp"),
        P("tp"),
        P("sp", "tp"),
        P(),
        P(None, "tp"),
        P(None, "tp"),
        P(),
        P(),
        P(),
        P(None, "tp"),
        P(None, "tp"),
        P(None, "tp"),
        P(None, "tp"),
        P("tp", None),
        P("tp", None),
    )
    return jax.shard_map(
        shards, mesh=mesh, in_specs=placed, out_specs=P(("sp", "tp"), None), check_vma=False
    )
```

profile of v0, /device:TPU:504, one launch (start us, length us, event | category | flops | bytes accessed | tf_op | source)
XLA Modules:
  0.0 570.1 jit_solution(10061996943856123440)
XLA Ops:
  10.1 4.3 all-to-all-start
  14.5 15.8 %all-to-all-done = bf16[8,256,256]{1,2,0:T(8,128)(2,1)S(1)} async-done(((bf16[8,256,256]{1,2,0:T(8,128)(2,1)}), bf16[8,256,256]{1,2,0:T(8,128)(2,1)S(1)}, u32[]{:S(2)}, u32[]{:S(2)}) %all-to-all-start) | async-done | bytes 1048608 | tf_op jit(solution)/shard_map/all_to_all | solution.py:36
  32.6 13.0 %all-gather.1 = bf16[196608]{0:T(1024)(128)(2,1)S(1)} all-gather(bf16[24576]{0:T(1024)(128)(2,1)S(1)} %pad_maximum_fusion.2), channel_id=3, replica_groups=mesh['sp'=64,'tp'=8] {'tp'}, dimensions={0}, use_global_device_ids=true | all-gather | bytes 442368 | tf_op jit(solution)/shard_map/all_gather | solution.py:60
  49.0 99.6 %all-gather.6.cloned.1.call-done = bf16[2048,768]{1,0:T(8,128)(2,1)} async-done(((bf16[32,768]{1,0:T(8,128)(2,1)}), bf16[2048,768]{1,0:T(8,128)(2,1)}) %all-gather.6.cloned.1.call-update) | async-done | bytes 3145744 | tf_op jit(solution)/shard_map/all_gather | solution.py:24
  148.6 3.2 fusion.31
  154.0 47.7 %while.44 = (s32[]{:T(128)}, f32[2,128,128]{2,1,0:T(8,128)S(1)}, f32[4,2,64,128]{3,2,0,1:T(8,128)}, f32[4,2,64,128]{3,1,2,0:T(2,128)S(1)}, f32[4,2,64,128]{3,1,2...) while((s32[]{:T(128)}, f32[2,128,128]{2,1,0:T(8,128)S(1)}, ...), condition=%wide.region_2.3_spmd.clone, body=%wide.region_0.2_spmd.clone.sunk | while | flops 80928768 | bytes 10721416 | solution.py:214
  156.2 8.2 %fusion.89 = f32[2,64,1,64]{3,2,1,0:T(1,128)S(1)} fusion(f32[2,64,128,1]{2,3,1,0:T(1,128)S(1)} %bitcast.167, f32[2,64,64,128]{3,2,1,0:T(8,128)S(1)} %multiply_multiply_fusion.2), kind=kOutput, calls=%fused_computation.27.clone.1 | convolution fusion | flops 12582912 | bytes 4292608 | tf_op jit(solution)/shard_map/while/body/eval_jaxpr/htsd,hsd->hts/dot_general | solution.py:111
  168.1 8.2 %fusion.89 = f32[2,64,1,64]{3,2,1,0:T(1,128)S(1)} fusion(f32[2,64,128,1]{2,3,1,0:T(1,128)S(1)} %bitcast.167, f32[2,64,64,128]{3,2,1,0:T(8,128)S(1)} %multiply_multiply_fusion.2), kind=kOutput, calls=%fused_computation.27.clone.1 | convolution fusion | flops 12582912 | bytes 4292608 | tf_op jit(solution)/shard_map/while/body/eval_jaxpr/htsd,hsd->hts/dot_general | solution.py:111
  180.0 8.2 %fusion.89 = f32[2,64,1,64]{3,2,1,0:T(1,128)S(1)} fusion(f32[2,64,128,1]{2,3,1,0:T(1,128)S(1)} %bitcast.167, f32[2,64,64,128]{3,2,1,0:T(8,128)S(1)} %multiply_multiply_fusion.2), kind=kOutput, calls=%fused_computation.27.clone.1 | convolution fusion | flops 12582912 | bytes 4292608 | tf_op jit(solution)/shard_map/while/body/eval_jaxpr/htsd,hsd->hts/dot_general | solution.py:111
  191.9 8.2 %fusion.89 = f32[2,64,1,64]{3,2,1,0:T(1,128)S(1)} fusion(f32[2,64,128,1]{2,3,1,0:T(1,128)S(1)} %bitcast.167, f32[2,64,64,128]{3,2,1,0:T(8,128)S(1)} %multiply_multiply_fusion.2), kind=kOutput, calls=%fused_computation.27.clone.1 | convolution fusion | flops 12582912 | bytes 4292608 | tf_op jit(solution)/shard_map/while/body/eval_jaxpr/htsd,hsd->hts/dot_general | solution.py:111
  210.1 81.1 %all_gather.23 = f32[64,2,128]{2,1,0:T(2,128)S(1)} all-gather(f32[1,2,128]{2,1,0:T(2,128)S(1)} %slice_exponential_fusion), channel_id=1, replica_groups=mesh['sp'=64,'tp'=8] {'sp'}, dimensions={0}, use_global_device_ids=true | all-gather | bytes 66560 | tf_op jit(solution)/shard_map/all_gather | solution.py:47
  291.6 29.4 %all-gather.8.cloned.1.call-done = bf16[16384,288]{0,1:T(8,128)(2,1)} async-done(((bf16[256,288]{0,1:T(8,128)(2,1)}), bf16[16384,288]{0,1:T(8,128)(2,1)}) %all-gather.8.cloned.1.call-update) | async-done | bytes 9437200 | tf_op jit(solution)/shard_map/all_gather | solution.py:24
  322.3 6.2 %fusion.48 = (bf16[16384,128]{0,1:T(8,128)(2,1)}, bf16[16384,128]{0,1:T(8,128)(2,1)}) fusion(bf16[16384,288]{0,1:T(8,128)(2,1)} %all-gather.8.cloned.1.call-done), kind=kLoop, calls=%fused_computation.117 | loop fusion | bytes 16777216 | tf_op jit(solution)/shard_map/split | solution.py:25
  328.6 129.9 %while.43 = (s32[]{:T(128)}, f32[2,256]{1,0:T(2,128)S(1)}, f32[2,256]{1,0:T(2,128)S(1)}, f32[2,256,64]{1,2,0:T(8,128)S(1)}, s32[]{:T(128)}, /*index=5*/bf16[1638...) while((s32[]{:T(128)}, f32[2,256]{1,0:T(2,128)S(1)}, ...), condition=%wide.region_16.17_spmd, body=%wide.region_11.16_spmd.sunk | while | flops 43420168 | bytes 3686729 | solution.py:290
  330.6 2.0 conditional.2
  336.7 2.0 conditional.2
  340.7 2.0 conditional.2
  387.4 2.0 conditional.2
  407.7 2.0 conditional.2
  432.1 2.0 conditional.2
  434.1 2.0 conditional.2
  458.5 15.1 %all-gather.10.cloned.1.call-done = f32[128,128,128]{2,1,0:T(8,128)} async-done(((f32[2,128,128]{2,1,0:T(8,128)}), f32[128,128,128]{2,1,0:T(8,128)}) %all-gather.10.cloned.1.call-update) | async-done | bytes 8388624 | tf_op jit(solution)/shard_map/all_gather | solution.py:47
  473.6 67.3 %while.42 = (s32[]{:T(128)}, f32[2,128,128]{2,1,0:T(8,128)S(1)}, s32[]{:T(128)}, f32[64,2,128]{2,1,0:T(2,128)S(1)}, f32[64,2,128,128]{3,2,1,0:T(8,128)}, /*index=5*/s32[]{:T(128)}, s32[]{:T(128)}, s32[]{:T(128)}) while((s32[]{:T(128)}, f32[2,128,128]{2,1,0:T(8,128)S(1)}, s32[]{:T(128)}, f32[64,2,128]{2,1,0:T(2,128)S(1)}, ...), condition=%wide.region_6.7_spmd, body=%wide.region_5.6_spmd.sunk | while | flops 65541 | bytes 396423 | solution.py:55
  542.5 20.3 %all_to_all.10 = bf16[8,32,2048]{2,1,0:T(8,128)(2,1)S(1)} all-to-all(bf16[8,32,2048]{2,1,0:T(8,128)(2,1)S(1)} %bitcast.171), channel_id=1, replica_groups=mesh['sp'=64,'tp'=8] {'tp'}, dimensions={0} | all-to-all | bytes 2097152 | tf_op jit(solution)/shard_map/all_to_all | solution.py:76
  (862 shorter events, 341.2 us)
Async XLA Ops:
  6.5 535.0 %copy-start = (bf16[256,2048]{1,0:T(8,128)(2,1)S(1)}, bf16[256,2048]{1,0:T(8,128)(2,1)}, u32[]{:S(2)}) copy-start(bf16[256,2048]{1,0:T(8,128)(2,1)} %param.42) | copy-start | bytes 3145732
  6.5 142.1 %all-gather.6.cloned.1.call-start = ((), (), s32[]{:S(2)}) async-start(), calls=%async_computation.2 | async-start | bytes 3194880 | tf_op jit(solution)/shard_map/all_gather | solution.py:24
  10.1 20.2 %all-to-all-start = ((bf16[8,256,256]{1,2,0:T(8,128)(2,1)}), bf16[8,256,256]{1,2,0:T(8,128)(2,1)S(1)}, u32[]{:S(2)}, u32[]{:S(2)}) async-start(bf16[8,256,256]{1,2,0:T(8,128)(2,1)} %broadcast_in_dim.83), calls=%async_computation | async-start | bytes 2097152 | tf_op jit(solution)/shard_map/all_to_all | solution.py:36
  14.4 33.1 %copy-start.14 = (f32[256]{0:T(256)S(1)}, f32[256]{0:T(256)}, u32[]{:S(2)}) copy-start(f32[256]{0:T(256)} %param.37) | copy-start | bytes 3076
  14.4 33.2 %copy-start.5 = (bf16[256,128]{1,0:T(8,128)(2,1)S(1)}, bf16[256,128]{1,0:T(8,128)(2,1)}, u32[]{:S(2)}) copy-start(bf16[256,128]{1,0:T(8,128)(2,1)} %param.41) | copy-start | bytes 196612
  14.4 33.5 %copy-start.6 = (bf16[256,128]{1,0:T(8,128)(2,1)S(1)}, bf16[256,128]{1,0:T(8,128)(2,1)}, u32[]{:S(2)}) copy-start(bf16[256,128]{1,0:T(8,128)(2,1)} %param.40) | copy-start | bytes 196612
  14.4 306.6 %all-gather.8.cloned.1.call-start = ((), (), s32[]{:S(2)}) async-start(), calls=%async_computation.3 | async-start | bytes 9584640 | tf_op jit(solution)/shard_map/all_gather | solution.py:24
  30.3 2.3 copy-start.2
  30.3 18.5 %copy-start.9 = (f32[256,2]{0,1:T(2,128)S(1)}, f32[256,2]{0,1:T(2,128)}, u32[]{:S(2)}) copy-start(f32[256,2]{0,1:T(2,128)} %param.31) | copy-start | bytes 6148
  30.3 18.7 %copy-start.12 = (f32[256]{0:T(256)S(1)}, f32[256]{0:T(256)}, u32[]{:S(2)}) copy-start(f32[256]{0:T(256)} %param.30) | copy-start | bytes 3076
  48.8 424.8 %all-gather.10.cloned.1.call-start = ((), (), s32[]{:S(2)}) async-start(), calls=%async_computation.4 | async-start | bytes 8519680 | tf_op jit(solution)/shard_map/all_gather | solution.py:47
  49.0 104.5 %copy-start.7 = (f32[2,128]{1,0:T(2,128)}, f32[2,128]{1,0:T(2,128)S(1)}, u32[]{:S(2)}) copy-start(f32[2,128]{1,0:T(2,128)S(1)} %bitcast_negate_fusion) | copy-start | bytes 3076
  49.0 104.5 %copy-start.13 = (f32[256]{0:T(256)S(1)}, f32[256]{0:T(256)}, u32[]{:S(2)}) copy-start(f32[256]{0:T(256)} %param.30) | copy-start | bytes 3076
  154.0 48.4 %copy-start.11 = (f32[512]{0:T(512)S(1)}, f32[512]{0:T(512)}, u32[]{:S(2)}) copy-start(f32[512]{0:T(512)} %param.36) | copy-start | bytes 6148
  201.7 0.7 copy-start.1
  203.5 5.7 copy-start.8
  203.6 5.7 copy-start.10
  205.2 4.8 copy-start.4
  328.5 212.9 %copy-start.15 = (f32[128]{0:T(128)S(1)}, f32[128]{0:T(128)}, u32[]{:S(2)}) copy-start(f32[128]{0:T(128)} %param.32) | copy-start | bytes 1540
  458.5 83.5 %copy-start.3 = (bf16[128,2048]{1,0:T(8,128)(2,1)S(1)}, bf16[128,2048]{1,0:T(8,128)(2,1)}, u32[]{:S(2)}) copy-start(bf16[128,2048]{1,0:T(8,128)(2,1)} %param.43) | copy-start | bytes 1572868
Sparse Core Ops, SparseCore 0:
  10.3 138.3 all-gather.5
  151.5 169.4 all-gather.7
  324.0 149.5 all-gather.9
where the time goes:
time: 575 us; the launch traced here: 570 us
  waiting for transfers between devices  160 us (28%)
  blocking collectives  114 us (20%)
  matrix products  99.5 us (17%)
  other arithmetic  93.4 us (16%)
  local copies, waits for them, and re-layouts  76.6 us (13%)
  between operations  13.7 us (2%)
  loops' own time  8.09 us (1%)
    all_gather x2, waiting for transfers between devices, side_by_side(): whole = lax.all_gather(both, axis, axis=dim, tiled=True)  129 us
    all_gather x1, blocking collectives, carried_in(): gathered = jax.tree.map(lambda a: lax.all_gather(a, axis), part)  81.1 us
    add x63, other arithmetic, chain_step(): later_part[0][..., None] * earlier[1] + later_part[1]  64.6 us
    dynamic_slice x64, local copies, waits for them, and re-layouts, visit(): lax.dynamic_slice_in_dim(value_piece, first_row, tok_dev, 0)  57 us
    dot_general x4, matrix products, block_step(): jnp.einsum('htsd,hsd->hts', queries[:, :, None, :] * decays, key_in, prec...  32.9 us
    all_to_all x1, blocking collectives, summed_on_arrival(): lax.all_to_all(in_blocks(value, dim, devices), axis, 0, 0, tiled=True)  20.3 us
    dot_general x64, matrix products, score_block(): jnp.einsum('qhr,kr->hqk', q_rope, k_rope, preferred_element_type=jnp.floa...  18.1 us
    dot_general x64, matrix products, score_block(): jnp.einsum('qhd,khd->hqk', q_nope, k_nope, preferred_element_type=jnp.flo...  17.1 us
  transfers between devices with their start and end apart: 4, of which 4 were waited for; matrix products, arithmetic and copies ran while one was open for 35% of the time, Pallas kernels for 0%

commit v1 on v0

v1 whole, which is shorter than its diff:
```python
import functools
import math

import jax
import jax.numpy as jnp
from jax import lax
from jax.experimental import pallas as pl
from jax.experimental.pallas import tpu as pltpu
from jax.sharding import PartitionSpec as P

HEAD = 128
NOPE = 64
ROPE = 32
NORM_EPS = 1e-06
ROPE_BASE = 10000.0
NEG_BIG = -1e30
NY = 4
CHUNK = 512
MESH = pl.DeviceIdType.MESH
F32 = jnp.float32
BF16 = jnp.bfloat16
NT = (((1,), (1,)), ((), ()))
TN = (((0,), (0,)), ((), ()))
VM = pltpu.VMEM
DMA = pltpu.SemaphoreType.DMA


def dot(a, b):
    return jnp.dot(a, b, preferred_element_type=F32)


def dotg(a, b, dims):
    return lax.dot_general(a, b, dims, preferred_element_type=F32)


def remote(src, dst, ssem, rsem, dev):
    return pltpu.make_async_remote_copy(
        src_ref=src, dst_ref=dst, send_sem=ssem, recv_sem=rsem, device_id=dev, device_id_type=MESH
    )


def take_bytes(ref, count, sem):
    part = ref.at[pl.ds(0, count)]
    pltpu.make_async_copy(part, part, sem).wait()


def lanes_of(shape):
    return lax.broadcasted_iota(jnp.int32, shape, len(shape) - 1)


class Line:
    def __init__(self, ref, ssem, rsem, nx):
        self.ref, self.ssem, self.rsem, self.nx = ref, ssem, rsem, nx
        tp = lax.axis_index("tp")
        self.tp, self.core, self.x = tp, lax.rem(tp, 2), tp // 2
        self.sib = self.x * 2 + 1 - self.core

    def at_x(self, dx):
        return lax.rem(self.x + dx + self.nx, self.nx) * 2 + self.core

    def copy(self, slot, to, k):
        piece = self.ref.at[slot]
        return remote(piece, piece, self.ssem, self.rsem.at[k], {"tp": to})

    def start(self):
        for d in range(1, self.nx):
            self.copy(self.tp, self.at_x(d), d - 1).start()
        self.copy(self.tp, self.sib, self.nx - 1).start()

    def forward(self):
        for d in range(1, self.nx):
            slot = self.at_x(-d)
            self.copy(slot, self.tp, d - 1).wait_recv()
            self.copy(slot, self.sib, self.nx - 1 + d).start()

    def finish(self):
        for d in range(self.nx):
            x = lax.rem(self.x - d + self.nx, self.nx)
            self.copy(x * 2 + 1 - self.core, self.tp, self.nx - 1 + d).wait_recv()

    def drain(self):
        take_bytes(self.ref, 2 * self.nx - 1, self.ssem)


class Plane:
    def __init__(self, ref, ssem, zsem, ysem, nz):
        self.ref, self.ssem, self.zsem, self.ysem, self.nz = ref, ssem, zsem, ysem, nz
        self.sp = lax.axis_index("sp")
        self.z, self.y = self.sp // NY, lax.rem(self.sp, NY)
        self.up, self.down = nz // 2, nz // 2 - 1

    def slot(self, dz, dy):
        z = lax.rem(self.z + dz + self.nz, self.nz)
        return z * NY + lax.rem(self.y + dy + NY, NY)

    def copy(self, slot, to, sem):
        piece = self.ref.at[slot]
        return remote(piece, piece, self.ssem, sem, {"sp": to})

    def ways(self, t):
        if t <= self.up:
            yield 1, t - 1, t < self.up
        if t <= self.down:
            yield -1, self.up + t - 1, t < self.down

    def drain(self):
        take_bytes(self.ref, self.nz * NY - 1, self.ssem)


class PlaneZY(Plane):
    def spread(self, slot):
        for d in range(1, NY):
            self.copy(slot, self.slot(0, d), self.ysem).start()

    def start(self):
        for way, k, _ in self.ways(1):
            self.copy(self.sp, self.slot(way, 0), self.zsem.at[k]).start()
        self.spread(self.sp)

    def step(self, t):
        for way, k, more in self.ways(t):
            slot = self.slot(-way * t, 0)
            self.copy(slot, self.sp, self.zsem.at[k]).wait_recv()
            if more:
                self.copy(slot, self.slot(way, 0), self.zsem.at[k + 1]).start()
            self.spread(slot)

    def finish(self):
        take_bytes(self.ref, self.nz * (NY - 1), self.ysem)


class PlaneYZ(Plane):
    def start(self):
        for d in range(1, NY):
            self.copy(self.sp, self.slot(0, d), self.ysem.at[d - 1]).start()
        self.launch(0)

    def launch(self, d):
        for way, k, _ in self.ways(1):
            self.copy(self.slot(0, -d), self.slot(way, 0), self.zsem.at[k, d]).start()

    def begin(self):
        for d in range(1, NY):
            self.copy(self.slot(0, -d), self.sp, self.ysem.at[d - 1]).wait_recv()
            self.launch(d)

    def step(self, t):
        for d in range(NY):
            for way, k, more in self.ways(t):
                slot = self.slot(-way * t, -d)
                self.copy(slot, self.sp, self.zsem.at[k, d]).wait_recv()
                if more:
                    self.copy(slot, self.slot(way, 0), self.zsem.at[k + 1, d]).start()


def gather_kernel(
    nz, nx, hid, wq, wf, wi, wqd, wkvd, wkr, wku, wvu, wqn, wqr, qg, kvg, kcos, ksin,
    left, qn, lat, kvw, qw,
    hall, wa, wb, rall, wr,
    loc, hs, hr, ks, kr, qs, qr, rs, rr, was, waz, way_, wbs, wbz, wby, ls, lz, ly,
):
    tpn, spn = 2 * nx, nz * NY
    tp, sp = lax.axis_index("tp"), lax.axis_index("sp")
    toks, feat = hid.shape
    tt = lat.shape[1]
    line_h, line_k = Line(hall, hs, hr, nx), Line(kvw, ks, kr, nx)
    line_q, line_r = Line(qw, qs, qr, nx), Line(rall, rs, rr, nx)
    plane_a = PlaneYZ(wa, was, waz, way_, nz)
    plane_b = PlaneZY(wb, wbs, wbz, wby, nz)
    plane_l = PlaneYZ(lat, ls, lz, ly, nz)

    barrier = pltpu.get_barrier_semaphore()
    greet = [{"tp": line_h.at_x(d)} for d in range(1, nx)] + [{"tp": line_h.sib}]
    greet += [{"sp": plane_a.slot(0, d)} for d in range(1, NY)]
    greet += [{"sp": plane_a.slot(1, 0)}, {"sp": plane_a.slot(-1, 0)}]
    for dev in greet:
        pl.semaphore_signal(barrier, inc=1, device_id=dev, device_id_type=MESH)

    own = [
        pltpu.make_async_copy(hid, hall.at[tp], loc.at[0]),
        pltpu.make_async_copy(wq, wa.at[sp], loc.at[1]),
        pltpu.make_async_copy(wf, wb.at[sp, :, pl.ds(0, wf.shape[1])], loc.at[2]),
        pltpu.make_async_copy(wi, wb.at[sp, :, pl.ds(wf.shape[1], wi.shape[1])], loc.at[3]),
        pltpu.make_async_copy(wku, kvw.at[tp, :, pl.ds(0, 128)], loc.at[4]),
        pltpu.make_async_copy(wvu, kvw.at[tp, :, pl.ds(128, 128)], loc.at[5]),
        pltpu.make_async_copy(wqn, qw.at[tp, :, pl.ds(0, 128)], loc.at[6]),
    ]
    for c in own:
        c.start()
    qw[tp, :, 128:256] = jnp.zeros((qw.shape[1], 128), BF16)
    qw[tp, :, 128:192] = wqr[...]
    wr[:, 0:64] = wqd[...]
    wr[:, 64:96] = wkvd[...]
    wr[:, 96:128] = wkr[...]
    for c in own:
        c.wait()
    pl.semaphore_wait(barrier, len(greet))

    line_h.start()
    plane_a.start()
    plane_b.start()
    line_k.start()
    plane_a.begin()

    def wstep(t):
        plane_b.step(t)
        plane_a.step(t)

    def lora():
        line_h.finish()
        acc = dot(hall[0], wr[0:feat, :])
        for i in range(1, tpn):
            acc = acc + dot(hall[i], wr[i * feat : (i + 1) * feat, :])
        rall[tp] = acc.astype(BF16)
        line_r.start()
        first = pl.multiple_of(tp * tt, tt)
        mine = dot(hall[0, pl.ds(first, tt), :], wr[0:feat, :])
        for i in range(1, tpn):
            mine = mine + dot(hall[i, pl.ds(first, tt), :], wr[i * feat : (i + 1) * feat, :])
        lane = lanes_of((tt, 128))
        other = jnp.where(
            lax.rem(lane, 32) < 16, pltpu.roll(mine, 128 - 16, 1), pltpu.roll(mine, 16, 1)
        )
        turned = mine * kcos[...] + other * ksin[...]
        both = jnp.where(
            lane < 32,
            pltpu.roll(turned, 32, 1),
            jnp.where(lane < 64, pltpu.roll(turned, 64, 1), 0.0),
        )
        lat[sp, :, 256:384] = both.astype(BF16)

    def latents():
        line_r.finish()
        lane = lanes_of((toks, 128))
        total = jnp.zeros((toks, 128), F32)
        for i in range(tpn):
            piece = rall[i].astype(F32)
            total = total + jnp.where(lane < 64, piece * piece, 0.0)
        width = 64 * tpn
        scale = lax.rsqrt(jnp.sum(total, axis=1, keepdims=True) / width + NORM_EPS)
        for j in range(width // 128):
            one, two = rall[2 * j].astype(F32), rall[2 * j + 1].astype(F32)
            tile = jnp.where(lane < 64, one, pltpu.roll(two, 64, 1))
            cols = slice(128 * j, 128 * (j + 1))
            qn[:, cols] = (tile * scale * qg[:, cols]).astype(BF16)
        first = pl.multiple_of(tp * tt, tt)
        lane = lanes_of((tt, 128))
        tiles = []
        total = jnp.zeros((tt, 128), F32)
        width = 32 * tpn
        for j in range(2):
            tile = jnp.zeros((tt, 128), F32)
            for k in range(4):
                if 4 * j + k >= tpn:
                    continue
                piece = rall[4 * j + k, pl.ds(first, tt), :].astype(F32)
                moved = pltpu.roll(piece, (32 * k - 64) % 128, 1) if k != 2 else piece
                tile = jnp.where((lane >= 32 * k) & (lane < 32 * (k + 1)), moved, tile)
            tiles.append(tile)
            total = total + tile * tile
        scale = lax.rsqrt(jnp.sum(total, axis=1, keepdims=True) / width + NORM_EPS)
        for j in range(2):
            cols = slice(128 * j, 128 * (j + 1))
            lat[sp, :, cols] = (tiles[j] * scale * kvg[:, cols]).astype(BF16)

    def project(w, cols, at):
        per = spn // tpn
        acc = None
        for i in range(tpn):
            block = w[i * per : (i + 1) * per, :, cols].reshape(feat, 256)
            part = dot(hall[i], block)
            acc = part if acc is None else acc + part
        left[:, at : at + 256] = acc.astype(BF16)

    last = nz // 2
    jobs = {
        2: [line_h.forward],
        3: [lora],
        4: [line_k.forward, line_r.forward],
        5: [latents, plane_l.start, line_q.start],
        6: [plane_l.begin],
    }
    lsteps = list(range(1, last + 1))
    for t in range(1, max(last, 6) + 1):
        if t <= last:
            wstep(t)
        for job in jobs.get(t, []):
            job()
        if t > 6:
            plane_l.step(lsteps.pop(0))
    plane_b.finish()
    tail = [
        lambda: project(wb, slice(0, 256), 256),
        lambda: project(wb, slice(256, 512), 512),
        lambda: project(wa, slice(0, 256), 0),
        line_q.forward,
    ]
    while lsteps or tail:
        if lsteps:
            plane_l.step(lsteps.pop(0))
        if tail:
            tail.pop(0)()
    line_k.finish()
    line_q.finish()
    for part in (line_h, line_k, line_q, line_r, plane_a, plane_b, plane_l):
        part.drain()


def scan_kernel(
    nz, leftr, gap, dex, lout, qx, into,
    stb, decb, ys, yd, zb, zdb, zs, zd, ib,
    ys_s, ys_r, yd_s, yd_r, zs_s, zs_r, zd_s, zd_r, i_s, i_r,
):
    sp = lax.axis_index("sp")
    z, y = sp // NY, lax.rem(sp, NY)
    toks = leftr.shape[0]
    half = toks // 2
    vs = HEAD // NY

    def at_y(d):
        return z * NY + lax.rem(y + d + NY, NY)

    def at_z(d):
        return lax.rem(z + d + nz, nz) * NY + y

    barrier = pltpu.get_barrier_semaphore()
    for d in range(1, NY):
        pl.semaphore_signal(barrier, inc=1, device_id={"sp": at_y(d)}, device_id_type=MESH)
    for d in range(1, nz):
        pl.semaphore_signal(barrier, inc=1, device_id={"sp": at_z(d)}, device_id_type=MESH)

    pre = leftr[:, 256:512].astype(F32)
    key = gap[...] * (1.0 / (1.0 + jnp.exp(pre)))
    series = jnp.full(key.shape, 1.0 / 11.0, F32)
    for n in range(10, 0, -1):
        series = series * key + 1.0 / n
    lane = lanes_of((toks, 256))
    logf = jnp.where(lane < 128, dex[:, 0:1], dex[:, 1:2]) - series * key
    rows = lax.broadcasted_iota(jnp.int32, (toks, toks), 0)
    lower = jnp.where(rows >= lanes_of((toks, toks)), 1.0, 0.0).astype(F32)
    cum = jnp.dot(lower, logf, preferred_element_type=F32, precision=lax.Precision.HIGHEST)
    qx[...] = (leftr[:, 0:256].astype(F32) * jnp.exp(cum)).astype(BF16)
    tri = lax.broadcasted_iota(jnp.int32, (half, half), 0) >= lanes_of((half, half))
    for h in range(2):
        cols = slice(HEAD * h, HEAD * (h + 1))
        c, k = cum[:, cols], key[:, cols]
        q = leftr[:, cols].astype(F32)
        v = leftr[:, 512 + HEAD * h : 512 + HEAD * (h + 1)]
        edge, last = c[half - 1 : half], c[toks - 1 : toks]
        outs = []
        for b in range(2):
            r = slice(half * b, half * (b + 1))
            mid = c[half * b + half // 2 - 1 : half * b + half // 2]
            qd = (q[r] * jnp.exp(c[r] - mid)).astype(BF16)
            kd = (k[r] * jnp.exp(mid - c[r])).astype(BF16)
            a = jnp.where(tri, dotg(qd, kd, NT), 0.0).astype(BF16)
            outs.append(dot(a, v[r]))
        s0 = dotg(v[:half], (k[:half] * jnp.exp(edge - c[:half])).astype(BF16), TN)
        qe = (q[half:] * jnp.exp(c[half:] - edge)).astype(BF16)
        lout[0:half, cols] = outs[0]
        lout[half:toks, cols] = outs[1] + dotg(qe, s0.astype(BF16), NT)
        st = dotg(v, (k * jnp.exp(last - c)).astype(BF16), TN)
        stb[h] = st.astype(BF16)
        decb[h : h + 1, :] = jnp.exp(last)
    pl.semaphore_wait(barrier, NY - 1 + nz - 1)

    def ycopy(d):
        to = lax.rem(y + d + NY, NY)
        mine = stb.at[:, pl.ds(pl.multiple_of(to * vs, vs), vs), :]
        dev = {"sp": at_y(d)}
        return (
            remote(mine, ys.at[y], ys_s.at[d - 1], ys_r.at[d - 1], dev),
            remote(decb, yd.at[y], yd_s.at[d - 1], yd_r.at[d - 1], dev),
        )

    def yarrive(d):
        src = lax.rem(y - d + NY, NY)
        dev = {"sp": sp}
        remote(ys.at[src], ys.at[src], ys_s.at[d - 1], ys_r.at[d - 1], dev).wait_recv()
        remote(yd.at[src], yd.at[src], yd_s.at[d - 1], yd_r.at[d - 1], dev).wait_recv()

    for d in range(1, NY):
        for c in ycopy(d):
            c.start()
    for h in range(2):
        ys[y, h] = stb[h, pl.ds(pl.multiple_of(y * vs, vs), vs), :]
    yd[y] = decb[...]
    for d in range(1, NY):
        yarrive(d)
    before, spans = [], []
    state = [jnp.zeros((vs, HEAD), F32) for _ in range(2)]
    span = [jnp.ones((1, HEAD), F32) for _ in range(2)]
    for j in range(NY):
        before.append(list(state))
        spans.append(list(span))
        for h in range(2):
            decay = yd[j, h : h + 1, :]
            state[h] = decay * state[h] + ys[j, h].astype(F32)
            span[h] = span[h] * decay
    for h in range(2):
        zb[h] = state[h].astype(BF16)
        zdb[h : h + 1, :] = span[h]

    def zcopy(d):
        dev = {"sp": (z + d) * NY + y}
        return (
            remote(zb, zs.at[z], zs_s.at[d - 1], zs_r.at[z], dev),
            remote(zdb, zd.at[z], zd_s.at[d - 1], zd_r.at[z], dev),
        )

    for d in range(1, nz):

        @pl.when(z + d < nz)
        def _():
            for c in zcopy(d):
                c.start()

    def earlier(j, carry):
        dev = {"sp": sp}
        remote(zs.at[j], zs.at[j], zs_s.at[0], zs_r.at[j], dev).wait_recv()
        remote(zd.at[j], zd.at[j], zd_s.at[0], zd_r.at[j], dev).wait_recv()
        return tuple(zd[j, h : h + 1, :] * carry[h] + zs[j, h].astype(F32) for h in range(2))

    zero = jnp.zeros((vs, HEAD), F32)
    carry = lax.fori_loop(0, z, earlier, (zero, zero))
    for j in range(NY):
        for h in range(2):
            ib[j, h] = (spans[j][h] * carry[h] + before[j][h]).astype(BF16)

    def icopy(d):
        to = lax.rem(y + d + NY, NY)
        spot = into.at[:, pl.ds(pl.multiple_of(y * vs, vs), vs), :]
        return remote(ib.at[to], spot, i_s.at[d - 1], i_r.at[d - 1], {"sp": at_y(d)})

    for d in range(1, NY):
        icopy(d).start()
    for h in range(2):
        into[h, pl.ds(pl.multiple_of(y * vs, vs), vs), :] = ib[y, h]
    for d in range(1, NY):
        src = lax.rem(y - d + NY, NY)
        spot = into.at[:, pl.ds(pl.multiple_of(src * vs, vs), vs), :]
        remote(spot, spot, i_s.at[d - 1], i_r.at[d - 1], {"sp": sp}).wait_recv()
    for d in range(1, NY):
        for c in ycopy(d):
            c.wait_send()
        icopy(d).wait_send()
    for d in range(1, nz):

        @pl.when(z + d < nz)
        def _():
            for c in zcopy(d):
                c.wait_send()


def attend_kernel(tpn, spn, qn, lat, kvw, qw, qcos, qsin, o, stats, qblk, msc, acc):
    sp, tp = lax.axis_index("sp"), lax.axis_index("tp")
    toks = qn.shape[0]
    tt = lat.shape[1]
    per = CHUNK // tt
    scale = 1.0 / math.sqrt(NOPE + ROPE)
    lane = lanes_of((toks, 128))
    stats_tile = jnp.zeros((toks, 128), F32)
    whole = sp // per

    def pair(p, stats_tile):
        q = dot(qn[...], qw[p])
        flat, turn = q[:, :128], q[:, 128:]
        other = jnp.where(
            lax.rem(lane, 32) < 16, pltpu.roll(turn, 128 - 16, 1), pltpu.roll(turn, 16, 1)
        )
        turn = turn * qcos[...] + other * qsin[...]
        qblk[0:toks, 0:128] = jnp.where(lane < 64, flat, 0.0).astype(BF16)
        qblk[toks:, 0:128] = jnp.where(lane < 64, 0.0, flat).astype(BF16)
        qblk[0:toks, 128:256] = jnp.where(lane < 32, turn, 0.0).astype(BF16)
        qblk[toks:, 128:256] = jnp.where((lane >= 32) & (lane < 64), turn, 0.0).astype(BF16)
        msc[...] = jnp.full((2 * toks, 128), NEG_BIG, F32)
        acc[...] = jnp.zeros((2 * toks, 256), F32)

        def chunk(j, masked):
            part = lat[pl.ds(j * per, per)].reshape(CHUNK, 384)
            kv = dot(part[:, : kvw.shape[1]], kvw[p]).astype(BF16)
            keys = jnp.concatenate([kv[:, :128], part[:, 256:]], axis=1)
            vals = jnp.concatenate([kv[:, 128:], jnp.ones((CHUNK, 128), BF16)], axis=1)
            for h in range(2):
                r = slice(h * toks, (h + 1) * toks)
                s = dotg(qblk[r, :], keys, NT)
                if masked:
                    at = lanes_of((toks, CHUNK))
                    kpos = (j * per + at // tt) * toks + tp * tt + lax.rem(at, tt)
                    qpos = sp * toks + lax.broadcasted_iota(jnp.int32, (toks, CHUNK), 0)
                    ok = kpos <= qpos
                    s = jnp.where(ok, s, NEG_BIG)
                old = msc[r, 0:1]
                new = jnp.maximum(old, jnp.max(s, axis=1, keepdims=True))
                w = jnp.exp((s - new) * scale)
                if masked:
                    w = jnp.where(ok, w, 0.0)
                fade = jnp.exp((old - new) * scale)
                acc[r, :] = acc[r, :] * fade + dot(w.astype(BF16), vals)
                msc[r, :] = jnp.broadcast_to(new, (toks, 128))

        @pl.loop(0, whole)
        def _(j):
            chunk(j, False)

        chunk(whole, True)
        outs = []
        for h in range(2):
            r = slice(h * toks, (h + 1) * toks)
            total = acc[r, 128:256]
            some = total > 0.0
            safe = jnp.where(some, total, 1.0)
            outs.append(acc[r, 0:128] / safe)
            lse = jnp.where(some, msc[r, :] * scale + jnp.log(safe), NEG_BIG)
            stats_tile = jnp.where(lane == 8 * p + h, lse, stats_tile)
        o[p] = jnp.where(lane < 64, outs[0], outs[1]).astype(BF16)
        return stats_tile

    stats_tile = lax.fori_loop(0, tpn, pair, stats_tile)
    stats[...] = jnp.transpose(stats_tile)[: stats.shape[0]]


def merge_kernel(
    nx, o, stats, lout, qx, into, gain, wor, woa, out,
    orecv, srecv, mixed, pairs, got_pair, sums, got,
    o_s, o_r, s_s, s_r, p_s, p_r, f_s, f_r,
):
    tpn = 2 * nx
    tp = lax.axis_index("tp")
    x, core = tp // 2, lax.rem(tp, 2)
    sib = x * 2 + 1 - core
    toks = lout.shape[0]
    tt = toks // tpn
    barrier = pltpu.get_barrier_semaphore()

    def at(d):
        return lax.rem(tp + d + tpn, tpn)

    for d in range(1, tpn):
        pl.semaphore_signal(barrier, inc=1, device_id={"tp": at(d)}, device_id_type=MESH)
    pl.semaphore_wait(barrier, tpn - 1)

    def parts(d):
        to = at(d)
        return (
            remote(o.at[to], orecv.at[tp], o_s.at[d - 1], o_r.at[d - 1], {"tp": to}),
            remote(stats.at[to], srecv.at[tp], s_s.at[d - 1], s_r.at[d - 1], {"tp": to}),
        )

    for d in range(1, tpn):
        for c in parts(d):
            c.start()
    orecv[tp] = o[tp]
    srecv[tp] = stats[tp]

    cols = []
    for h in range(2):
        c = slice(HEAD * h, HEAD * (h + 1))
        raw = lout[:, c] + dotg(qx[:, c], into[h], NT)
        norm = lax.rsqrt(jnp.mean(raw * raw, axis=1, keepdims=True) + NORM_EPS)
        cols.append((raw * norm * gain[...]).astype(BF16))
    rec = jnp.concatenate(cols, axis=1)
    width = wor.shape[1]
    step = 512
    for n in range(0, width, step):
        mixed[:, n : n + step] = dot(rec, wor[:, n : n + step])

    for d in range(1, tpn):
        src = at(-d)
        dev = {"tp": tp}
        remote(orecv.at[src], orecv.at[src], o_s.at[d - 1], o_r.at[d - 1], dev).wait_recv()
        remote(srecv.at[src], srecv.at[src], s_s.at[d - 1], s_r.at[d - 1], dev).wait_recv()
    rowsT = srecv[...].reshape(8 * tpn, toks)
    if 8 * tpn < 128:
        rowsT = jnp.concatenate([rowsT, jnp.zeros((128 - 8 * tpn, toks), F32)], axis=0)
    lse = jnp.transpose(rowsT)
    lane = lanes_of((toks, 128))
    top = [
        functools.reduce(jnp.maximum, [lse[:, 8 * i + h : 8 * i + h + 1] for i in range(tpn)])
        for h in range(2)
    ]
    total = jnp.zeros((toks, 128), F32)
    merged = jnp.zeros((toks, 128), F32)
    for i in range(tpn):
        both = [jnp.exp(lse[:, 8 * i + h : 8 * i + h + 1] - top[h]) for h in range(2)]
        weight = jnp.where(lane < 64, both[0], both[1])
        total = total + weight
        merged = merged + weight * orecv[i].astype(F32)
    att = (merged / total).astype(BF16)
    for n in range(0, width, step):
        mixed[:, n : n + step] += dot(att, woa[:, n : n + step])

    for i in range(nx):
        first = pl.multiple_of((2 * i + 1 - core) * tt, tt)
        pairs[i] = mixed[pl.ds(first, tt), :].astype(BF16)
    pair = remote(pairs, got_pair, p_s, p_r, {"tp": sib})
    pair.start()
    pair.wait_recv()

    def mine(i):
        first = pl.multiple_of((2 * i + core) * tt, tt)
        return mixed[pl.ds(first, tt), :] + got_pair[i].astype(F32)

    def final(d):
        i = lax.rem(x + d, nx)
        return remote(sums.at[d - 1], got.at[d - 1], f_s.at[d - 1], f_r.at[d - 1], {"tp": i * 2 + core})

    for d in range(1, nx):
        sums[d - 1] = mine(lax.rem(x + d, nx)).astype(BF16)
        final(d).start()
    total = mine(x)
    for d in range(1, nx):
        final(d).wait_recv()
        total = total + got[d - 1].astype(F32)
    out[...] = total.astype(BF16)
    pair.wait_send()
    for d in range(1, nx):
        final(d).wait_send()
    for d in range(1, tpn):
        for c in parts(d):
            c.wait_send()


def call(kernel, name, ins, outs, scratch, cid=None):
    params = {"vmem_limit_bytes": 60 * 2**20}
    if cid is not None:
        params |= {"collective_id": cid, "has_side_effects": True}
    return pl.pallas_call(
        kernel,
        out_shape=[jax.ShapeDtypeStruct(s, d) for s, d in outs],
        in_specs=[pl.BlockSpec(memory_space=VM)] * ins,
        out_specs=[pl.BlockSpec(memory_space=VM)] * len(outs),
        scratch_shapes=scratch,
        compiler_params=pltpu.CompilerParams(**params),
        name=name,
    )


def shards(
    nz, nx,
    hidden_in, w_query_rec, w_forget, w_input, forget_gap, decay_extra, rec_gain,
    w_q_down, w_kv_down, w_key_rope, q_gain, kv_gain, w_q_nope, w_q_rope, w_k_up, w_v_up,
    w_out_rec, w_out_att,
):
    tpn, spn = 2 * nx, nz * NY
    toks, feat = hidden_in.shape
    tt = toks // tpn
    rw = w_query_rec.shape[0]
    qrank = w_q_down.shape[1] * tpn
    sp, tp = lax.axis_index("sp"), lax.axis_index("tp")

    position = (sp * toks + jnp.arange(toks)).astype(F32)
    lane = jnp.arange(128)
    frequency = 1.0 / ROPE_BASE ** (jnp.arange(0, ROPE, 2, dtype=F32) / ROPE)
    angle = position[:, None] * frequency[None, :]
    sign = jnp.where(lane % 32 < 16, -1.0, 1.0).astype(F32)
    qcos = jnp.tile(jnp.cos(angle), (1, 8))
    qsin = jnp.tile(jnp.sin(angle), (1, 8)) * sign[None, :]
    kcos = lax.dynamic_slice_in_dim(qcos, tp * tt, tt, 0)
    ksin = lax.dynamic_slice_in_dim(qsin, tp * tt, tt, 0)
    kvg = jnp.pad(kv_gain, (0, 256 - kv_gain.shape[0]))

    line = [DMA(()), DMA((2 * nx - 1,))]
    yz = [DMA(()), DMA((nz - 1, NY)), DMA((NY - 1,))]
    left, qn, lat, kvw, qw = call(
        functools.partial(gather_kernel, nz, nx),
        "gather",
        15,
        [
            ((toks, 768), BF16),
            ((toks, qrank), BF16),
            ((spn, tt, 384), BF16),
            ((tpn, w_k_up.shape[0], 256), BF16),
            ((tpn, qrank, 256), BF16),
        ],
        [
            VM((tpn, toks, feat), BF16),
            VM((spn, rw, 256), BF16),
            VM((spn, rw, 512), BF16),
            VM((tpn, toks, 128), BF16),
            VM((tpn * feat, 128), BF16),
            DMA((7,)),
            *line, *line, *line, *line,
            *yz, DMA(()), DMA((nz - 1,)), DMA(()), *yz,
        ],
        cid=0,
    )(
        hidden_in, w_query_rec, w_forget, w_input, w_q_down, w_kv_down, w_key_rope,
        w_k_up, w_v_up, w_q_nope, w_q_rope, q_gain[None], kvg[None], kcos, ksin,
    )

    vs = HEAD // NY
    lout, qx, into = call(
        functools.partial(scan_kernel, nz),
        "scan",
        3,
        [((toks, 256), F32), ((toks, 256), BF16), ((2, HEAD, HEAD), BF16)],
        [
            VM((2, HEAD, HEAD), BF16),
            VM((8, HEAD), F32),
            VM((NY, 2, vs, HEAD), BF16),
            VM((NY, 8, HEAD), F32),
            VM((2, vs, HEAD), BF16),
            VM((8, HEAD), F32),
            VM((nz, 2, vs, HEAD), BF16),
            VM((nz, 8, HEAD), F32),
            VM((NY, 2, vs, HEAD), BF16),
            *([DMA((NY - 1,))] * 4),
            DMA((nz - 1,)), DMA((nz,)), DMA((nz - 1,)), DMA((nz,)),
            *([DMA((NY - 1,))] * 2),
        ],
        cid=1,
    )(left, forget_gap[None], decay_extra)

    o, stats = call(
        functools.partial(attend_kernel, tpn, spn),
        "attend",
        6,
        [((tpn, toks, 128), BF16), ((8 * tpn, toks), F32)],
        [VM((2 * toks, 256), BF16), VM((2 * toks, 128), F32), VM((2 * toks, 256), F32)],
    )(qn, lat, kvw, qw, qcos, qsin)

    (out,) = call(
        functools.partial(merge_kernel, nx),
        "merge",
        8,
        [((tt, w_out_rec.shape[1]), BF16)],
        [
            VM((tpn, toks, 128), BF16),
            VM((tpn, 8, toks), F32),
            VM((toks, w_out_rec.shape[1]), F32),
            VM((nx, tt, w_out_rec.shape[1]), BF16),
            VM((nx, tt, w_out_rec.shape[1]), BF16),
            VM((max(nx - 1, 1), tt, w_out_rec.shape[1]), BF16),
            VM((max(nx - 1, 1), tt, w_out_rec.shape[1]), BF16),
            *([DMA((tpn - 1,))] * 4),
            DMA(()), DMA(()),
            *([DMA((max(nx - 1, 1),))] * 2),
        ],
        cid=2,
    )(o, stats.reshape(tpn, 8, toks), lout, qx, into, rec_gain[None], w_out_rec, w_out_att)
    return out


def solution(mesh):
    placed = (
        P("sp", "tp"),
        P("sp", "tp"),
        P("sp", "tp"),
        P("sp", "tp"),
        P("tp"),
        P("sp", "tp"),
        P(),
        P(None, "tp"),
        P(None, "tp"),
        P(),
        P(),
        P(),
        P(None, "tp"),
        P(None, "tp"),
        P(None, "tp"),
        P(None, "tp"),
        P("tp", None),
        P("tp", None),
    )
    nz, nx = mesh.shape["sp"] // NY, mesh.shape["tp"] // 2
    return jax.shard_map(
        functools.partial(shards, nz, nx),
        mesh=mesh,
        in_specs=placed,
        out_specs=P(("sp", "tp"), None),
        check_vma=False,
    )
```

time: 575 us -> 171 us (0.30)
  the two profiles are of different devices: /device:TPU:504 before, /device:TPU:448 now
where the time goes in v1:
time: 171 us
  Pallas kernels  162 us (95%)
  local copies, waits for them, and re-layouts  8.02 us (5%)
    pallas_call x1, Pallas kernels, shards(): call(functools.partial(gather_kernel, nz, nx), 'gather', 15, [((toks, 768...  63.2 us
    pallas_call x1, Pallas kernels, shards(): call(functools.partial(attend_kernel, tpn, spn), 'attend', 6, [((tpn, tok...  42.2 us
    pallas_call x1, Pallas kernels, shards(): call(functools.partial(scan_kernel, nz), 'scan', 3, [((toks, 256), F32),...  31.7 us
    pallas_call x1, Pallas kernels, shards(): call(functools.partial(merge_kernel, nx), 'merge', 8, [((tt, w_out_rec.sh...  25.3 us
    unnamed x18, local copies, waits for them, and re-layouts  7.16 us

profile of v1, /device:TPU:448, one launch (start us, length us, event | category | flops | bytes accessed | tf_op | source)
XLA Modules:
  0.0 170.8 jit_solution(6300394669779109986)
XLA Ops:
  0.0 0.0 copy-start.3
  0.0 0.1 multiply_sine_fusion
  0.2 0.1 copy.25
  0.3 0.0 copy-start
  0.4 0.1 copy.24.qcos
  0.5 0.0 copy-start.1
  0.5 0.7 constant_dynamic-slice_fusion
  1.1 2.0 %copy.26.wqd = bf16[2048,64]{1,0:T(8,128)(2,1)} copy(bf16[2048,64]{0,1:T(8,128)(2,1)} %param.25) | data formatting | bytes 524288 | tf_op args[7]
  3.1 0.0 copy-done.2
  3.1 1.0 copy.27.wkvd
  4.1 0.0 copy-done.3
  4.1 1.0 copy.28.wkr
  5.1 0.0 copy-done.4
  5.1 0.8 copy.29.wqr
  5.9 63.2 %gather.1 = (bf16[256,768]{1,0:T(8,128)(2,1)}, bf16[256,512]{1,0:T(8,128)(2,1)}, bf16[64,32,384]{2,1,0:T(8,128)(2,1)}, bf16[8,256,256]{2,1,0:T(8,128)(2,1)}, bf16[8,512,256]{2,1,0:T(8,128)(2,1)}) custom-call(bf16[256,256]{1,0:T(8,128)(2,1)} %hid.1, bf16[32,256]{1,0:T(8,128)(2,1)} %wq.1, bf16[32,256]{1,0:T(8,128)(2,1)} %wf.1, bf16[32,256]{1,0:T(8,128)(2,1)} %wi.1, ...), custom_call_target="tpu_custom_call" | custom-call | tf_op jit(solution)/shard_map/gather/pallas_call | solution.py:665
  69.2 0.0 copy-done
  69.2 0.0 copy-done.1
  69.2 0.0 copy-start.5
  69.2 42.2 %attend.1 = (bf16[8,256,128]{2,1,0:T(8,128)(2,1)}, f32[64,256]{1,0:T(8,128)}) custom-call(bf16[256,512]{1,0:T(8,128)(2,1)} %get-tuple-element.15.qn, bf16[64,32,384]{2,1,0:T(8,128)(2,1)} %get-tuple-element.16.lat, bf16[8,256,256]{2,1,0:T(8,128)(2,1)} %get-tuple-element.17.kvw, bf16[8,512,256]{2,1,0:T(8,128)(2,1)} %get-tuple-element.18.qw, ...), custom_call_target="tpu_custom_call" | custom-call | tf_op jit(solution)/shard_map/attend/pallas_call | solution.py:715
  111.4 0.0 copy-done.5
  111.4 0.8 copy.31.dex
  112.2 31.7 %scan.1 = (f32[256,256]{1,0:T(8,128)}, bf16[256,256]{1,0:T(8,128)(2,1)}, bf16[2,128,128]{2,1,0:T(8,128)(2,1)}) custom-call(bf16[256,768]{1,0:T(8,128)(2,1)} %get-tuple-element.21.leftr, f32[1,256]{1,0:T(1,128)} %bitcast.12, f32[256,2]{1,0:T(8,128)} %copy.31.dex), custom_call_target="tpu_custom_call" | custom-call | tf_op jit(solution)/shard_map/scan/pallas_call | solution.py:693
  143.9 25.3 %merge.1 = bf16[32,2048]{1,0:T(8,128)(2,1)} custom-call(bf16[8,256,128]{2,1,0:T(8,128)(2,1)} %get-tuple-element.19.o, f32[8,8,256]{2,1,0:T(8,128)} %bitcast.9, f32[256,256]{1,0:T(8,128)} %get-tuple-element.22.lout, bf16[256,256]{1,0:T(8,128)(2,1)} %get-tuple-element.23.qx, bf16[2,128,128]{2,1,0:T(8,128)(2,1)} %get-tuple-element.24.into, f32[1,128]{1,0:T(1,128)} %bitcast.13, ...), custom_call_target="tpu_custom_call" | custom-call | tf_op jit(solution)/shard_map/merge/pallas_call | solution.py:723
  169.2 1.6 copy.33
  (8 shorter events, 0.1 us)
Async XLA Ops:
  0.0 3.1 %copy-start.2 = (bf16[2048,32]{0,1:T(8,128)(2,1)S(1)}, bf16[2048,32]{0,1:T(8,128)(2,1)}, u32[]{:S(2)}) copy-start(bf16[2048,32]{0,1:T(8,128)(2,1)} %param.26) | copy-start | bytes 393220
  0.0 4.1 %copy-start.3 = (bf16[2048,32]{0,1:T(8,128)(2,1)S(1)}, bf16[2048,32]{0,1:T(8,128)(2,1)}, u32[]{:S(2)}) copy-start(bf16[2048,32]{0,1:T(8,128)(2,1)} %param.27) | copy-start | bytes 393220
  0.0 5.1 %copy-start.4 = (bf16[512,64]{0,1:T(8,128)(2,1)S(1)}, bf16[512,64]{0,1:T(8,128)(2,1)}, u32[]{:S(2)}) copy-start(bf16[512,64]{0,1:T(8,128)(2,1)} %param.31) | copy-start | bytes 196612
  0.3 68.8 %copy-start = (f32[256,128]{1,0:T(8,128)}, f32[256,128]{1,0:T(8,128)S(1)}, u32[]{:S(2)}) copy-start(f32[256,128]{1,0:T(8,128)S(1)} %broadcast_multiply_fusion.qsin) | copy-start | bytes 393220
  0.5 68.7 %copy-start.1 = (f32[256,128]{1,0:T(8,128)}, f32[256,128]{1,0:T(8,128)S(1)}, u32[]{:S(2)}) copy-start(f32[256,128]{1,0:T(8,128)S(1)} %copy.24.qcos) | copy-start | bytes 393220
  69.2 42.2 %copy-start.5 = (f32[256,2]{0,1:T(2,128)S(1)}, f32[256,2]{0,1:T(2,128)}, u32[]{:S(2)}) copy-start(f32[256,2]{0,1:T(2,128)} %param.23) | copy-start | bytes 6148

commit v2 on v1

v2 whole, which is shorter than its diff:
```python
import functools
import math

import jax
import jax.numpy as jnp
from jax import lax
from jax.experimental import pallas as pl
from jax.experimental.pallas import tpu as pltpu
from jax.sharding import PartitionSpec as P

HEAD = 128
NOPE = 64
ROPE = 32
NORM_EPS = 1e-06
ROPE_BASE = 10000.0
NEG_BIG = -1e30
NY = 4
CHUNK = 512
SPLIT = 4
FULL_GREET = False
MESH = pl.DeviceIdType.MESH
F32 = jnp.float32
BF16 = jnp.bfloat16
NT = (((1,), (1,)), ((), ()))
TN = (((0,), (0,)), ((), ()))
VM = pltpu.VMEM
DMA = pltpu.SemaphoreType.DMA


def dot(a, b):
    return jnp.dot(a, b, preferred_element_type=F32)


def dotg(a, b, dims):
    return lax.dot_general(a, b, dims, preferred_element_type=F32)


def remote(src, dst, ssem, rsem, dev):
    return pltpu.make_async_remote_copy(
        src_ref=src, dst_ref=dst, send_sem=ssem, recv_sem=rsem, device_id=dev, device_id_type=MESH
    )


def take_bytes(ref, count, sem):
    part = ref.at[pl.ds(0, count)]
    pltpu.make_async_copy(part, part, sem).wait()


def lanes_of(shape):
    return lax.broadcasted_iota(jnp.int32, shape, len(shape) - 1)


class Line:
    def __init__(self, ref, ssem, rsem, nx):
        self.ref, self.ssem, self.rsem, self.nx = ref, ssem, rsem, nx
        tp = lax.axis_index("tp")
        self.tp, self.core, self.x = tp, lax.rem(tp, 2), tp // 2
        self.sib = self.x * 2 + 1 - self.core

    def at_x(self, dx):
        return lax.rem(self.x + dx + self.nx, self.nx) * 2 + self.core

    def copy(self, slot, to, k):
        piece = self.ref.at[slot]
        return remote(piece, piece, self.ssem, self.rsem.at[k], {"tp": to})

    def start(self):
        for d in range(1, self.nx):
            self.copy(self.tp, self.at_x(d), d - 1).start()
        self.copy(self.tp, self.sib, self.nx - 1).start()

    def forward(self):
        for d in range(1, self.nx):
            slot = self.at_x(-d)
            self.copy(slot, self.tp, d - 1).wait_recv()
            self.copy(slot, self.sib, self.nx - 1 + d).start()

    def finish(self):
        for d in range(self.nx):
            x = lax.rem(self.x - d + self.nx, self.nx)
            self.copy(x * 2 + 1 - self.core, self.tp, self.nx - 1 + d).wait_recv()

    def drain(self):
        take_bytes(self.ref, 2 * self.nx - 1, self.ssem)


class Plane:
    def __init__(self, ref, ssem, zsem, ysem, nz):
        self.ref, self.ssem, self.zsem, self.ysem, self.nz = ref, ssem, zsem, ysem, nz
        self.sp = lax.axis_index("sp")
        self.z, self.y = self.sp // NY, lax.rem(self.sp, NY)
        self.limit = {1: nz // 2, -1: nz // 2 - 1}
        self.steps = (nz // 2 + 1) // 2

    def slot(self, dz, dy):
        z = lax.rem(self.z + dz + self.nz, self.nz)
        return z * NY + lax.rem(self.y + dy + NY, NY)

    def copy(self, slot, to, sem):
        piece = self.ref.at[slot]
        return remote(piece, piece, self.ssem, sem, {"sp": to})

    def next_of(self, way, d):
        return [c for c in (d + 2, d + 1) if d % 2 == 0 and c <= self.limit[way]]

    def key(self, way, d):
        return d - 1 if way == 1 else self.limit[1] + d - 1

    def arrivals(self, t):
        return [(w, d) for d in (2 * t - 1, 2 * t) for w in (1, -1) if d <= self.limit[w]]

    def drain(self):
        take_bytes(self.ref, self.nz * NY - 1, self.ssem)


class PlaneZY(Plane):
    def hand_on(self, way, d):
        for c in self.next_of(way, d):
            self.copy(self.slot(-way * d, 0), self.slot(way * (c - d), 0), self.zsem.at[self.key(way, c)]).start()

    def spread(self, slot):
        for d in range(1, NY):
            self.copy(slot, self.slot(0, d), self.ysem).start()

    def start(self):
        self.hand_on(1, 0)
        self.hand_on(-1, 0)
        self.spread(self.sp)

    def step(self, t):
        for way, d in self.arrivals(t):
            slot = self.slot(-way * d, 0)
            self.copy(slot, self.sp, self.zsem.at[self.key(way, d)]).wait_recv()
            self.hand_on(way, d)
            self.spread(slot)

    def finish(self):
        take_bytes(self.ref, self.nz * (NY - 1), self.ysem)


class PlaneYZ(Plane):
    def hand_on(self, way, d, j):
        for c in self.next_of(way, d):
            sem = self.zsem.at[self.key(way, c), j]
            self.copy(self.slot(-way * d, -j), self.slot(way * (c - d), 0), sem).start()

    def start(self):
        for d in range(1, NY):
            self.copy(self.sp, self.slot(0, d), self.ysem.at[d - 1]).start()
        self.hand_on(1, 0, 0)
        self.hand_on(-1, 0, 0)

    def begin(self):
        for j in range(1, NY):
            self.copy(self.slot(0, -j), self.sp, self.ysem.at[j - 1]).wait_recv()
            self.hand_on(1, 0, j)
            self.hand_on(-1, 0, j)

    def step(self, t):
        for way, d in self.arrivals(t):
            for j in range(NY):
                slot = self.slot(-way * d, -j)
                self.copy(slot, self.sp, self.zsem.at[self.key(way, d), j]).wait_recv()
                self.hand_on(way, d, j)


class Scan:
    def __init__(self, nz, left, gap, dext, lout, qx, into, key, cum, stb, decb, ys, yd, zb, zdb, zs, zd, ib, sems):
        self.nz = nz
        self.left, self.gap, self.dext, self.lout, self.qx, self.into = left, gap, dext, lout, qx, into
        self.key, self.cum = key, cum
        self.stb, self.decb, self.ys, self.yd = stb, decb, ys, yd
        self.zb, self.zdb, self.zs, self.zd, self.ib = zb, zdb, zs, zd, ib
        self.ys_s, self.ys_r, self.yd_s, self.yd_r, self.zs_s, self.zs_r, self.zd_s, self.zd_r, self.i_s, self.i_r = sems
        self.sp = lax.axis_index("sp")
        self.z, self.y = self.sp // NY, lax.rem(self.sp, NY)
        self.vs = HEAD // NY

    def at_y(self, d):
        return self.z * NY + self.other(d)

    def other(self, d):
        return lax.rem(self.y + d + NY, NY)

    def rows(self, ref, j):
        return ref.at[:, pl.ds(pl.multiple_of(j * self.vs, self.vs), self.vs), :]

    def prepare(self):
        toks = self.left.shape[0]
        pre = self.left[:, 256:512].astype(F32)
        key = self.gap[...] * (1.0 / (1.0 + jnp.exp(pre)))
        series = jnp.full(key.shape, 1.0 / 11.0, F32)
        for n in range(10, 0, -1):
            series = series * key + 1.0 / n
        extra = [jnp.transpose(jnp.broadcast_to(self.dext[h : h + 1, :], (HEAD, toks))) for h in range(2)]
        logf = jnp.concatenate(extra, axis=1) - series * key
        rows = lax.broadcasted_iota(jnp.int32, (toks, toks), 0)
        lower = jnp.where(rows >= lanes_of((toks, toks)), 1.0, 0.0).astype(F32)
        cum = jnp.dot(lower, logf, preferred_element_type=F32, precision=lax.Precision.HIGHEST)
        self.qx[...] = (self.left[:, 0:256].astype(F32) * jnp.exp(cum)).astype(BF16)
        self.key[...] = key
        self.cum[...] = cum

    def local(self):
        toks = self.left.shape[0]
        half = toks // 2
        tri = lax.broadcasted_iota(jnp.int32, (half, half), 0) >= lanes_of((half, half))
        for h in range(2):
            cols = slice(HEAD * h, HEAD * (h + 1))
            c, k = self.cum[:, cols], self.key[:, cols]
            v = self.left[:, 512 + HEAD * h : 512 + HEAD * (h + 1)]
            last = c[toks - 1 : toks]
            self.stb[h] = dotg(v, (k * jnp.exp(last - c)).astype(BF16), TN).astype(BF16)
            self.decb[h : h + 1, :] = jnp.exp(last)
        for d in range(1, NY):
            for c in self.ycopy(d):
                c.start()
        for h in range(2):
            cols = slice(HEAD * h, HEAD * (h + 1))
            c, k = self.cum[:, cols], self.key[:, cols]
            q = self.left[:, cols].astype(F32)
            v = self.left[:, 512 + HEAD * h : 512 + HEAD * (h + 1)]
            edge = c[half - 1 : half]
            outs = []
            for b in range(2):
                r = slice(half * b, half * (b + 1))
                mid = c[half * b + half // 2 - 1 : half * b + half // 2]
                qd = (q[r] * jnp.exp(c[r] - mid)).astype(BF16)
                kd = (k[r] * jnp.exp(mid - c[r])).astype(BF16)
                a = jnp.where(tri, dotg(qd, kd, NT), 0.0).astype(BF16)
                outs.append(dot(a, v[r]))
            s0 = dotg(v[:half], (k[:half] * jnp.exp(edge - c[:half])).astype(BF16), TN)
            qe = (q[half:] * jnp.exp(c[half:] - edge)).astype(BF16)
            self.lout[0:half, cols] = outs[0]
            self.lout[half:toks, cols] = outs[1] + dotg(qe, s0.astype(BF16), NT)

    def ycopy(self, d):
        mine = self.rows(self.stb, self.other(d))
        dev = {"sp": self.at_y(d)}
        return (
            remote(mine, self.ys.at[self.y], self.ys_s.at[d - 1], self.ys_r.at[d - 1], dev),
            remote(self.decb, self.yd.at[self.y], self.yd_s.at[d - 1], self.yd_r.at[d - 1], dev),
        )

    def join_y(self):
        dev = {"sp": self.sp}
        y, ys, yd = self.y, self.ys, self.yd
        for h in range(2):
            ys[y, h] = self.stb[h, pl.ds(pl.multiple_of(y * self.vs, self.vs), self.vs), :]
        yd[y] = self.decb[...]
        for d in range(1, NY):
            src = self.other(-d)
            remote(ys.at[src], ys.at[src], self.ys_s.at[d - 1], self.ys_r.at[d - 1], dev).wait_recv()
            remote(yd.at[src], yd.at[src], self.yd_s.at[d - 1], self.yd_r.at[d - 1], dev).wait_recv()
        state = [jnp.zeros((self.vs, HEAD), F32) for _ in range(2)]
        span = [jnp.ones((1, HEAD), F32) for _ in range(2)]
        for j in range(NY):
            for h in range(2):
                decay = yd[j, h : h + 1, :]
                state[h] = decay * state[h] + ys[j, h].astype(F32)
                span[h] = span[h] * decay
        for h in range(2):
            self.zb[h] = state[h].astype(BF16)
            self.zdb[h : h + 1, :] = span[h]
        for d in range(1, self.nz):

            @pl.when(self.z + d < self.nz)
            def _():
                for c in self.zcopy(d):
                    c.start()

    def zcopy(self, d):
        dev = {"sp": (self.z + d) * NY + self.y}
        return (
            remote(self.zb, self.zs.at[self.z], self.zs_s.at[d - 1], self.zs_r.at[self.z], dev),
            remote(self.zdb, self.zd.at[self.z], self.zd_s.at[d - 1], self.zd_r.at[self.z], dev),
        )

    def join_z(self):
        zs, zd, ys, yd = self.zs, self.zd, self.ys, self.yd
        dev = {"sp": self.sp}

        def earlier(j, carry):
            remote(zs.at[j], zs.at[j], self.zs_s.at[0], self.zs_r.at[j], dev).wait_recv()
            remote(zd.at[j], zd.at[j], self.zd_s.at[0], self.zd_r.at[j], dev).wait_recv()
            return tuple(zd[j, h : h + 1, :] * carry[h] + zs[j, h].astype(F32) for h in range(2))

        zero = jnp.zeros((self.vs, HEAD), F32)
        state = list(lax.fori_loop(0, self.z, earlier, (zero, zero)))
        for j in range(NY):
            for h in range(2):
                self.ib[j, h] = state[h].astype(BF16)
                state[h] = yd[j, h : h + 1, :] * state[h] + ys[j, h].astype(F32)
        for d in range(1, NY):
            self.icopy(d).start()
        for h in range(2):
            spot = pl.ds(pl.multiple_of(self.y * self.vs, self.vs), self.vs)
            self.into[h, spot, :] = self.ib[self.y, h]

    def icopy(self, d):
        spot = self.rows(self.into, self.y)
        return remote(self.ib.at[self.other(d)], spot, self.i_s.at[d - 1], self.i_r.at[d - 1], {"sp": self.at_y(d)})

    def finish(self):
        for d in range(1, NY):
            spot = self.rows(self.into, self.other(-d))
            remote(spot, spot, self.i_s.at[d - 1], self.i_r.at[d - 1], {"sp": self.sp}).wait_recv()

    def drain(self):
        for d in range(1, NY):
            for c in self.ycopy(d):
                c.wait_send()
            self.icopy(d).wait_send()
        for d in range(1, self.nz):

            @pl.when(self.z + d < self.nz)
            def _():
                for c in self.zcopy(d):
                    c.wait_send()


def mixer_kernel(
    nz, nx, hid, wq, wf, wi, wqdt, wkvdt, wkrt, wku, wvu, wqn, wqrt, qg, kvg, kcos, ksin, qcos, qsin,
    gap, dext, gain, worh, woah, out,
    hall, wa, wb, rall, racc, wrt, left, qn, lat, kvw, qw, wor, woa,
    lout, qx, into, key, cum, stb, decb, ys, yd, zb, zdb, zs, zd, ib,
    qblk, msc, acc, obuf, sbuf, orecv, srecv, mixed, pairs, got_pair, sums, got,
    loc, hs, hr, ks, kr, qs, qr, rs, rr, was, waz, way_, wbs, wbz, wby, ls, lz, ly,
    ys_s, ys_r, yd_s, yd_r, zs_s, zs_r, zd_s, zd_r, i_s, i_r,
    o_s, o_r, s_s, s_r, p_s, p_r, f_s, f_r,
):
    tpn, spn = 2 * nx, nz * NY
    tp, sp = lax.axis_index("tp"), lax.axis_index("sp")
    x, core = tp // 2, lax.rem(tp, 2)
    toks, feat = hid.shape
    tt = lat.shape[1]
    line_h, line_k = Line(hall, hs, hr, nx), Line(kvw, ks, kr, nx)
    line_q, line_r = Line(qw, qs, qr, nx), Line(rall, rs, rr, nx)
    plane_a = PlaneYZ(wa, was, waz, way_, nz)
    plane_b = PlaneZY(wb, wbs, wbz, wby, nz)
    plane_l = PlaneZY(lat, ls, lz, ly, nz)
    sems = (ys_s, ys_r, yd_s, yd_r, zs_s, zs_r, zd_s, zd_r, i_s, i_r)
    scan = Scan(nz, left, gap, dext, lout, qx, into, key, cum, stb, decb, ys, yd, zb, zdb, zs, zd, ib, sems)

    barrier = pltpu.get_barrier_semaphore()
    greet = [{"tp": lax.rem(tp + d, tpn)} for d in range(1, tpn)]
    greet += [{"sp": plane_a.slot(0, d)} for d in range(1, NY)]
    near = [d for d in range(1, nz) if FULL_GREET or d <= 2 or d >= nz - 2]
    greet += [{"sp": plane_a.slot(d, 0)} for d in near]
    for dev in greet:
        pl.semaphore_signal(barrier, inc=1, device_id=dev, device_id_type=MESH)

    own = [
        pltpu.make_async_copy(hid, hall.at[tp], loc.at[0]),
        pltpu.make_async_copy(wq, wa.at[sp], loc.at[1]),
        pltpu.make_async_copy(wf, wb.at[sp, :, pl.ds(0, wf.shape[1])], loc.at[2]),
        pltpu.make_async_copy(wi, wb.at[sp, :, pl.ds(wf.shape[1], wi.shape[1])], loc.at[3]),
        pltpu.make_async_copy(wku, kvw.at[tp, :, pl.ds(0, 128)], loc.at[4]),
        pltpu.make_async_copy(wvu, kvw.at[tp, :, pl.ds(128, 128)], loc.at[5]),
    ]
    late = [pltpu.make_async_copy(worh, wor, loc.at[6]), pltpu.make_async_copy(woah, woa, loc.at[7])]
    for c in own + late:
        c.start()
    wrt[0:64, :] = wqdt[...]
    wrt[64:96, :] = wkvdt[...]
    wrt[96:128, :] = wkrt[...]
    for c in own:
        c.wait()
    pl.semaphore_wait(barrier, len(greet))

    line_h.start()
    plane_a.start()
    plane_b.start()
    line_k.start()
    qw[tp, 0:128, :] = jnp.transpose(wqn[...].astype(F32)).astype(BF16)
    qw[tp, 128:192, :] = wqrt[...]
    qblk[...] = jnp.zeros(qblk.shape, BF16)
    plane_a.begin()

    def wstep(t):
        plane_b.step(t)
        plane_a.step(t)

    def lora():
        line_h.finish()
        acc = None
        for i in range(tpn):
            part = dotg(hall[i], wrt[:, i * feat : (i + 1) * feat], NT)
            acc = part if acc is None else acc + part
        rall[tp] = acc.astype(BF16)
        line_r.start()
        racc[...] = acc
        mine = racc[pl.ds(pl.multiple_of(tp * tt, tt), tt), :]
        lane = lanes_of((tt, 128))
        other = jnp.where(
            lax.rem(lane, 32) < 16, pltpu.roll(mine, 128 - 16, 1), pltpu.roll(mine, 16, 1)
        )
        turned = mine * kcos[...] + other * ksin[...]
        lat[sp, :, 256:384] = jnp.where(lane < 32, pltpu.roll(turned, 32, 1), 0.0).astype(BF16)

    def latents():
        line_r.finish()
        first = pl.multiple_of(tp * tt, tt)
        lane = lanes_of((tt, 128))
        tiles = []
        total = jnp.zeros((tt, 128), F32)
        width = 32 * tpn
        for j in range(2):
            tile = jnp.zeros((tt, 128), F32)
            for k in range(4):
                if 4 * j + k >= tpn:
                    continue
                piece = rall[4 * j + k, pl.ds(first, tt), :].astype(F32)
                moved = pltpu.roll(piece, (32 * k - 64) % 128, 1) if k != 2 else piece
                tile = jnp.where((lane >= 32 * k) & (lane < 32 * (k + 1)), moved, tile)
            tiles.append(tile)
            total = total + tile * tile
        scale = lax.rsqrt(jnp.sum(total, axis=1, keepdims=True) / width + NORM_EPS)
        for j in range(2):
            cols = slice(128 * j, 128 * (j + 1))
            lat[sp, :, cols] = (tiles[j] * scale * kvg[:, cols]).astype(BF16)

    def queries():
        lane = lanes_of((toks, 128))
        total = jnp.zeros((toks, 128), F32)
        for i in range(tpn):
            piece = rall[i].astype(F32)
            total = total + jnp.where(lane < 64, piece * piece, 0.0)
        width = 64 * tpn
        scale = lax.rsqrt(jnp.sum(total, axis=1, keepdims=True) / width + NORM_EPS)
        for j in range(width // 128):
            one, two = rall[2 * j].astype(F32), rall[2 * j + 1].astype(F32)
            tile = jnp.where(lane < 64, one, pltpu.roll(two, 64, 1))
            cols = slice(128 * j, 128 * (j + 1))
            qn[:, cols] = (tile * scale * qg[:, cols]).astype(BF16)

    def project(w, cols, at):
        per = spn // tpn
        acc = None
        for i in range(tpn):
            block = w[i * per : (i + 1) * per, :, cols].reshape(feat, 256)
            part = dot(hall[i], block)
            acc = part if acc is None else acc + part
        left[:, at : at + 256] = acc.astype(BF16)

    jobs = {
        1: [line_h.forward],
        2: [lora, line_k.forward],
        3: [line_r.forward, latents, plane_l.start, line_q.start],
        4: [queries],
    }
    lsteps = list(range(1, plane_l.steps + 1))
    for t in range(1, max(plane_a.steps, 4) + 1):
        if t <= plane_a.steps:
            wstep(t)
        for job in jobs.get(t, []):
            job()
    if lsteps:
        plane_l.step(lsteps.pop(0))
    plane_b.finish()
    tail = [
        lambda: (project(wb, slice(0, 256), 256), project(wb, slice(256, 512), 512)),
        lambda: project(wa, slice(0, 256), 0),
        scan.prepare,
        scan.local,
        line_q.forward,
    ]
    while lsteps or tail:
        if tail:
            tail.pop(0)()
        if lsteps:
            plane_l.step(lsteps.pop(0))
    scan.join_y()
    line_k.finish()
    line_q.finish()
    plane_l.finish()

    per = CHUNK // tt
    base2 = math.log2(math.e) / math.sqrt(NOPE + ROPE)
    whole = sp // per

    def sent(p):
        dev = {"tp": p}
        return (
            remote(obuf.at[p], orecv.at[tp], o_s.at[p], o_r.at[tp], dev),
            remote(sbuf.at[p], srecv.at[tp], s_s.at[p], s_r.at[tp], dev),
        )

    def pair(i, _):
        p = lax.rem(tp + 1 + i, tpn)
        q = dotg(qw[p], qn[...], NT)
        for h in range(2):
            c = slice(h * toks, (h + 1) * toks)
            qblk[64 * h : 64 * (h + 1), c] = q[64 * h : 64 * (h + 1)].astype(BF16)
            a, b = q[128 + 32 * h : 144 + 32 * h], q[144 + 32 * h : 160 + 32 * h]
            qblk[128:144, c] = (a * qcos[...] - b * qsin[...]).astype(BF16)
            qblk[144:160, c] = (a * qsin[...] + b * qcos[...]).astype(BF16)
        msc[...] = jnp.full(msc.shape, NEG_BIG, F32)
        acc[...] = jnp.zeros(acc.shape, F32)

        def chunk(j, masked):
            part = lat[pl.ds(j * per, per)].reshape(CHUNK, 384)
            kv = dot(part[:, : kvw.shape[1]], kvw[p])
            keys = jnp.concatenate([kv[:, :128].astype(BF16), part[:, 256:]], axis=1)
            vals = jnp.transpose(kv[:, 128:]).astype(BF16)
            vals = jnp.concatenate([vals, jnp.ones((16, CHUNK), BF16)], axis=0)
            for h in range(2):
                c = slice(h * toks, (h + 1) * toks)
                s = dot(keys, qblk[:, c])
                if masked:
                    at = lax.broadcasted_iota(jnp.int32, (CHUNK, toks), 0)
                    kpos = (j * per + at // tt) * toks + tp * tt + lax.rem(at, tt)
                    ok = kpos <= sp * toks + lanes_of((CHUNK, toks))
                    s = jnp.where(ok, s, NEG_BIG)
                old = msc[0:1, c]
                new = jnp.maximum(old, jnp.max(s, axis=0, keepdims=True))
                w = jnp.exp2((s - new) * base2)
                if masked:
                    w = jnp.where(ok, w, 0.0)
                fade = jnp.exp2((old - new) * base2)
                acc[:, c] = acc[:, c] * fade + dot(vals, w.astype(BF16))
                msc[0:1, c] = new

        @pl.loop(0, whole)
        def _(j):
            chunk(j, False)

        chunk(whole, True)
        for h in range(2):
            c = slice(h * toks, (h + 1) * toks)
            total = acc[128:129, c]
            some = total > 0.0
            safe = jnp.where(some, total, 1.0)
            obuf[p, 64 * h : 64 * (h + 1), :] = (acc[64 * h : 64 * (h + 1), c] / safe).astype(BF16)
            sbuf[p, h : h + 1, :] = jnp.where(some, msc[0:1, c] * base2 + jnp.log2(safe), NEG_BIG)

        @pl.when(i < tpn - 1)
        def _():
            for c in sent(p):
                c.start()

        return 0

    lax.fori_loop(0, tpn - 2, pair, 0)
    scan.join_z()
    lax.fori_loop(tpn - 2, tpn, pair, 0)
    orecv[tp] = obuf[tp]
    srecv[tp] = sbuf[tp]

    scan.finish()
    cols = []
    for h in range(2):
        c = slice(HEAD * h, HEAD * (h + 1))
        raw = lout[:, c] + dotg(qx[:, c], into[h], NT)
        norm = lax.rsqrt(jnp.mean(raw * raw, axis=1, keepdims=True) + NORM_EPS)
        cols.append((raw * norm * gain[...]).astype(BF16))
    rec = jnp.concatenate(cols, axis=1)
    for c in late:
        c.wait()
    width = wor.shape[1]
    step = got.shape[3]
    for n in range(0, width, step):
        mixed[:, n : n + step] = dot(rec, wor[:, n : n + step])

    for d in range(1, tpn):
        src = lax.rem(tp + d, tpn)
        dev = {"tp": tp}
        remote(orecv.at[src], orecv.at[src], o_s.at[src], o_r.at[src], dev).wait_recv()
        remote(srecv.at[src], srecv.at[src], s_s.at[src], s_r.at[src], dev).wait_recv()
    halves = []
    for h in range(2):
        lse = [srecv[i, h : h + 1, :] for i in range(tpn)]
        top = functools.reduce(jnp.maximum, lse)
        total = jnp.zeros((1, toks), F32)
        merged = jnp.zeros((64, toks), F32)
        for i in range(tpn):
            weight = jnp.exp2(lse[i] - top)
            total = total + weight
            merged = merged + weight * orecv[i, 64 * h : 64 * (h + 1), :].astype(F32)
        halves.append((merged / total).astype(BF16))
    att = jnp.concatenate(halves, axis=0)

    sib = x * 2 + 1 - core

    def to_sib(k):
        return remote(pairs.at[k], got_pair.at[k], p_s.at[k], p_r.at[k], {"tp": sib})

    for k in range(width // step):
        n = slice(k * step, (k + 1) * step)
        mixed[:, n] += dotg(att, woa[:, n], TN)
        for i in range(nx):
            first = pl.multiple_of((2 * i + 1 - core) * tt, tt)
            pairs[k, i] = mixed[pl.ds(first, tt), n].astype(BF16)
        to_sib(k).start()

    def mine(i, k):
        first = pl.multiple_of((2 * i + core) * tt, tt)
        return mixed[pl.ds(first, tt), k * step : (k + 1) * step] + got_pair[k, i].astype(F32)

    def final(d, k):
        to = lax.rem(x + d, nx) * 2 + core
        return remote(sums.at[k, d - 1], got.at[k, d - 1], f_s.at[k, d - 1], f_r.at[k, d - 1], {"tp": to})

    for k in range(width // step):
        to_sib(k).wait_recv()
        for d in range(1, nx):
            sums[k, d - 1] = mine(lax.rem(x + d, nx), k).astype(BF16)
            final(d, k).start()
    for k in range(width // step):
        total = mine(x, k)
        for d in range(1, nx):
            final(d, k).wait_recv()
            total = total + got[k, d - 1].astype(F32)
        out[:, k * step : (k + 1) * step] = total.astype(BF16)
    for k in range(width // step):
        to_sib(k).wait_send()
        for d in range(1, nx):
            final(d, k).wait_send()
    for d in range(1, tpn):
        for c in sent(lax.rem(tp + d, tpn)):
            c.wait_send()
    for part in (line_h, line_k, line_q, line_r, plane_a, plane_b, plane_l, scan):
        part.drain()


def shards(
    nz, nx,
    hidden_in, w_query_rec, w_forget, w_input, forget_gap, decay_extra, rec_gain,
    w_q_down, w_kv_down, w_key_rope, q_gain, kv_gain, w_q_nope, w_q_rope, w_k_up, w_v_up,
    w_out_rec, w_out_att,
):
    tpn, spn = 2 * nx, nz * NY
    toks, feat = hidden_in.shape
    tt = toks // tpn
    rw = w_query_rec.shape[0]
    qrank = w_q_down.shape[1] * tpn
    kvrank = w_k_up.shape[0]
    width = w_out_rec.shape[1]
    sp, tp = lax.axis_index("sp"), lax.axis_index("tp")

    frequency = 1.0 / ROPE_BASE ** (jnp.arange(0, ROPE, 2, dtype=F32) / ROPE)
    position = (sp * toks + jnp.arange(toks)).astype(F32)
    angle = frequency[:, None] * position[None, :]
    qcos, qsin = jnp.cos(angle), jnp.sin(angle)
    keyed = (sp * toks + tp * tt + jnp.arange(tt)).astype(F32)
    angle = keyed[:, None] * jnp.tile(frequency, 8)[None, :]
    sign = jnp.where(jnp.arange(128) % 32 < 16, -1.0, 1.0).astype(F32)
    kcos, ksin = jnp.cos(angle), jnp.sin(angle) * sign[None, :]
    kvg = jnp.pad(kv_gain, (0, 256 - kv_gain.shape[0]))

    vs = HEAD // NY
    step = width // SPLIT
    line = [DMA(()), DMA((2 * nx - 1,))]
    far = max(nx - 1, 1)
    scratch = [
        VM((tpn, toks, feat), BF16),
        VM((spn, rw, 256), BF16),
        VM((spn, rw, 512), BF16),
        VM((tpn, toks, 128), BF16),
        VM((toks, 128), F32),
        VM((128, tpn * feat), BF16),
        VM((toks, 768), BF16),
        VM((toks, qrank), BF16),
        VM((spn, tt, 384), BF16),
        VM((tpn, kvrank, 256), BF16),
        VM((tpn, 192, qrank), BF16),
        VM(w_out_rec.shape, BF16),
        VM(w_out_att.shape, BF16),
        VM((toks, 256), F32),
        VM((toks, 256), BF16),
        VM((2, HEAD, HEAD), BF16),
        VM((toks, 256), F32),
        VM((toks, 256), F32),
        VM((2, HEAD, HEAD), BF16),
        VM((8, HEAD), F32),
        VM((NY, 2, vs, HEAD), BF16),
        VM((NY, 8, HEAD), F32),
        VM((2, vs, HEAD), BF16),
        VM((8, HEAD), F32),
        VM((nz, 2, vs, HEAD), BF16),
        VM((nz, 8, HEAD), F32),
        VM((NY, 2, vs, HEAD), BF16),
        VM((256, 2 * toks), BF16),
        VM((8, 2 * toks), F32),
        VM((144, 2 * toks), F32),
        VM((tpn, 128, toks), BF16),
        VM((tpn, 8, toks), F32),
        VM((tpn, 128, toks), BF16),
        VM((tpn, 8, toks), F32),
        VM((toks, width), F32),
        VM((SPLIT, nx, tt, step), BF16),
        VM((SPLIT, nx, tt, step), BF16),
        VM((SPLIT, far, tt, step), BF16),
        VM((SPLIT, far, tt, step), BF16),
        DMA((8,)),
        *line, *line, *line, *line,
        DMA(()), DMA((nz - 1, NY)), DMA((NY - 1,)),
        DMA(()), DMA((nz - 1,)), DMA(()),
        DMA(()), DMA((nz - 1,)), DMA(()),
        *([DMA((NY - 1,))] * 4),
        DMA((nz - 1,)), DMA((nz,)), DMA((nz - 1,)), DMA((nz,)),
        *([DMA((NY - 1,))] * 2),
        *([DMA((tpn,))] * 4),
        *([DMA((SPLIT,))] * 2),
        *([DMA((SPLIT, far))] * 2),
    ]
    args = (
        hidden_in, w_query_rec, w_forget, w_input, w_q_down.T, w_kv_down.T, w_key_rope.T,
        w_k_up, w_v_up, w_q_nope, w_q_rope.T, q_gain[None], kvg[None], kcos, ksin, qcos, qsin,
        forget_gap[None], decay_extra.T, rec_gain[None], w_out_rec, w_out_att,
    )
    whole, anywhere = pl.BlockSpec(memory_space=VM), pl.BlockSpec(memory_space=pl.ANY)
    return pl.pallas_call(
        functools.partial(mixer_kernel, nz, nx),
        out_shape=jax.ShapeDtypeStruct((tt, width), BF16),
        in_specs=[whole] * (len(args) - 2) + [anywhere] * 2,
        out_specs=whole,
        scratch_shapes=scratch,
        compiler_params=pltpu.CompilerParams(
            collective_id=0, has_side_effects=True, vmem_limit_bytes=60 * 2**20
        ),
        name="mixer",
    )(*args)


def solution(mesh):
    placed = (
        P("sp", "tp"),
        P("sp", "tp"),
        P("sp", "tp"),
        P("sp", "tp"),
        P("tp"),
        P("sp", "tp"),
        P(),
        P(None, "tp"),
        P(None, "tp"),
        P(),
        P(),
        P(),
        P(None, "tp"),
        P(None, "tp"),
        P(None, "tp"),
        P(None, "tp"),
        P("tp", None),
        P("tp", None),
    )
    nz, nx = mesh.shape["sp"] // NY, mesh.shape["tp"] // 2
    return jax.shard_map(
        functools.partial(shards, nz, nx),
        mesh=mesh,
        in_specs=placed,
        out_specs=P(("sp", "tp"), None),
        check_vma=False,
    )
```

time: 171 us -> 103 us (0.60)
  the two profiles are of different devices: /device:TPU:448 before, /device:TPU:385 now
where the time goes in v2:
time: 103 us
  Pallas kernels  99.9 us (97%)
  local copies, waits for them, and re-layouts  1.65 us (2%)
  other arithmetic  1.54 us (1%)
    pallas_call x1, Pallas kernels, shards(): pl.pallas_call(functools.partial(mixer_kernel, nz, nx), out_shape=jax.Sha...  99.9 us

profile of v2, /device:TPU:385, one launch (start us, length us, event | category | flops | bytes accessed | tf_op | source)
XLA Modules:
  0.0 103.1 jit_solution(18015778187842746095)
XLA Ops:
  0.0 0.1 mul.47
  0.1 0.8 fusion
  0.9 0.8 multiply_sine_fusion
  1.6 99.9 %mixer.1 = bf16[32,2048]{1,0:T(8,128)(2,1)} custom-call(bf16[256,256]{1,0:T(8,128)(2,1)} %hid.1, bf16[32,256]{1,0:T(8,128)(2,1)} %wq.1, bf16[32,256]{1,0:T(8,128)(2,1)} %wf.1, bf16[32,256]{1,0:T(8,128)(2,1)} %wi.1, bf16[64,2048]{1,0:T(8,128)(2,1)} %bitcast.9, bf16[32,2048]{1,0:T(8,128)(2,1)} %bitcast.10, bf16[32,2048]{1,0:T(8,128)(2,1)} %bitcast.11, ...), custom_call_target="tpu_custom_call" | custom-call | tf_op jit(solution)/shard_map/mixer/pallas_call | solution.py:713
  101.5 1.6 %copy.20 = bf16[32,2048]{1,0:T(8,128)(2,1)} copy(bf16[32,2048]{1,0:T(8,128)(2,1)} %mixer.1) | data formatting | bytes 262144
  (5 shorter events, 0.0 us)

commit v3 on v2

--- a/solution.py
+++ b/solution.py
@@ -118,24 +118,26 @@
         for c in self.next_of(way, d):
             self.copy(self.slot(-way * d, 0), self.slot(way * (c - d), 0), self.zsem.at[self.key(way, c)]).start()
 
-    def spread(self, slot):
+    def spread(self, slot, t):
         for d in range(1, NY):
-            self.copy(slot, self.slot(0, d), self.ysem).start()
+            self.copy(slot, self.slot(0, d), self.ysem.at[t]).start()
 
     def start(self):
         self.hand_on(1, 0)
         self.hand_on(-1, 0)
-        self.spread(self.sp)
+        self.spread(self.sp, 0)
 
     def step(self, t):
         for way, d in self.arrivals(t):
             slot = self.slot(-way * d, 0)
             self.copy(slot, self.sp, self.zsem.at[self.key(way, d)]).wait_recv()
             self.hand_on(way, d)
-            self.spread(slot)
-
-    def finish(self):
-        take_bytes(self.ref, self.nz * (NY - 1), self.ysem)
+            self.spread(slot, t)
+
+    def finish(self, first, last):
+        for t in range(first, last + 1):
+            count = len(self.arrivals(t)) if t else 1
+            take_bytes(self.ref, count * (NY - 1), self.ysem.at[t])
 
 
 class PlaneYZ(Plane):
@@ -197,14 +199,11 @@
         rows = lax.broadcasted_iota(jnp.int32, (toks, toks), 0)
         lower = jnp.where(rows >= lanes_of((toks, toks)), 1.0, 0.0).astype(F32)
         cum = jnp.dot(lower, logf, preferred_element_type=F32, precision=lax.Precision.HIGHEST)
-        self.qx[...] = (self.left[:, 0:256].astype(F32) * jnp.exp(cum)).astype(BF16)
         self.key[...] = key
         self.cum[...] = cum
 
-    def local(self):
+    def states(self):
         toks = self.left.shape[0]
-        half = toks // 2
-        tri = lax.broadcasted_iota(jnp.int32, (half, half), 0) >= lanes_of((half, half))
         for h in range(2):
             cols = slice(HEAD * h, HEAD * (h + 1))
             c, k = self.cum[:, cols], self.key[:, cols]
@@ -215,6 +214,12 @@
         for d in range(1, NY):
             for c in self.ycopy(d):
                 c.start()
+
+    def inside(self):
+        toks = self.left.shape[0]
+        half = toks // 2
+        tri = lax.broadcasted_iota(jnp.int32, (half, half), 0) >= lanes_of((half, half))
+        self.qx[...] = (self.left[:, 0:256].astype(F32) * jnp.exp(self.cum[...])).astype(BF16)
         for h in range(2):
             cols = slice(HEAD * h, HEAD * (h + 1))
             c, k = self.cum[:, cols], self.key[:, cols]
@@ -262,7 +267,7 @@
         for h in range(2):
             self.zb[h] = state[h].astype(BF16)
             self.zdb[h : h + 1, :] = span[h]
-        for d in range(1, self.nz):
+        for d in range(self.nz - 1, 0, -1):
 
             @pl.when(self.z + d < self.nz)
             def _():
@@ -322,10 +327,10 @@
 def mixer_kernel(
     nz, nx, hid, wq, wf, wi, wqdt, wkvdt, wkrt, wku, wvu, wqn, wqrt, qg, kvg, kcos, ksin, qcos, qsin,
     gap, dext, gain, worh, woah, out,
-    hall, wa, wb, rall, racc, wrt, left, qn, lat, kvw, qw, wor, woa,
+    hall, wa, wb, wc, rall, racc, wrt, left, qn, lat, kvw, qw, wor, woa,
     lout, qx, into, key, cum, stb, decb, ys, yd, zb, zdb, zs, zd, ib,
-    qblk, msc, acc, obuf, sbuf, orecv, srecv, mixed, pairs, got_pair, sums, got,
-    loc, hs, hr, ks, kr, qs, qr, rs, rr, was, waz, way_, wbs, wbz, wby, ls, lz, ly,
+    krope, qblk, msc, acc, obuf, sbuf, orecv, srecv, mixed, pairs, got_pair, sums, got,
+    loc, hs, hr, ks, kr, qs, qr, rs, rr, was, waz, way_, wbs, wbz, wby, wcs, wcz, wcy, ls, lz, ly,
     ys_s, ys_r, yd_s, yd_r, zs_s, zs_r, zd_s, zd_r, i_s, i_r,
     o_s, o_r, s_s, s_r, p_s, p_r, f_s, f_r,
 ):
@@ -333,11 +338,12 @@
     tp, sp = lax.axis_index("tp"), lax.axis_index("sp")
     x, core = tp // 2, lax.rem(tp, 2)
     toks, feat = hid.shape
-    tt = lat.shape[1]
+    tt = toks // tpn
     line_h, line_k = Line(hall, hs, hr, nx), Line(kvw, ks, kr, nx)
     line_q, line_r = Line(qw, qs, qr, nx), Line(rall, rs, rr, nx)
     plane_a = PlaneYZ(wa, was, waz, way_, nz)
     plane_b = PlaneZY(wb, wbs, wbz, wby, nz)
+    plane_c = PlaneYZ(wc, wcs, wcz, wcy, nz)
     plane_l = PlaneZY(lat, ls, lz, ly, nz)
     sems = (ys_s, ys_r, yd_s, yd_r, zs_s, zs_r, zd_s, zd_r, i_s, i_r)
     scan = Scan(nz, left, gap, dext, lout, qx, into, key, cum, stb, decb, ys, yd, zb, zdb, zs, zd, ib, sems)
@@ -352,9 +358,10 @@
 
     own = [
         pltpu.make_async_copy(hid, hall.at[tp], loc.at[0]),
-        pltpu.make_async_copy(wq, wa.at[sp], loc.at[1]),
-        pltpu.make_async_copy(wf, wb.at[sp, :, pl.ds(0, wf.shape[1])], loc.at[2]),
-        pltpu.make_async_copy(wi, wb.at[sp, :, pl.ds(wf.shape[1], wi.shape[1])], loc.at[3]),
+        pltpu.make_async_copy(wf.at[:, pl.ds(0, 128)], wa.at[sp], loc.at[1]),
+        pltpu.make_async_copy(wf.at[:, pl.ds(128, 128)], wb.at[sp, :, pl.ds(0, 128)], loc.at[2]),
+        pltpu.make_async_copy(wi, wb.at[sp, :, pl.ds(128, 256)], loc.at[3]),
+        pltpu.make_async_copy(wq, wc.at[sp], loc.at[8]),
         pltpu.make_async_copy(wku, kvw.at[tp, :, pl.ds(0, 128)], loc.at[4]),
         pltpu.make_async_copy(wvu, kvw.at[tp, :, pl.ds(128, 128)], loc.at[5]),
     ]
@@ -389,6 +396,7 @@
             acc = part if acc is None else acc + part
         rall[tp] = acc.astype(BF16)
         line_r.start()
+        line_q.start()
         racc[...] = acc
         mine = racc[pl.ds(pl.multiple_of(tp * tt, tt), tt), :]
         lane = lanes_of((tt, 128))
@@ -396,7 +404,14 @@
             lax.rem(lane, 32) < 16, pltpu.roll(mine, 128 - 16, 1), pltpu.roll(mine, 16, 1)
         )
         turned = mine * kcos[...] + other * ksin[...]
-        lat[sp, :, 256:384] = jnp.where(lane < 32, pltpu.roll(turned, 32, 1), 0.0).astype(BF16)
+        quart = tt // 4
+        lane = lanes_of((quart, 128))
+        packed = jnp.zeros((quart, 128), F32)
+        for g in range(4):
+            rows = turned[g * quart : (g + 1) * quart]
+            moved = pltpu.roll(rows, 32 * (g + 1), 1) if g < 3 else rows
+            packed = jnp.where((lane >= 32 * g) & (lane < 32 * (g + 1)), moved, packed)
+        lat[sp, 2 * tt : 2 * tt + quart, :] = packed.astype(BF16)
 
     def latents():
         line_r.finish()
@@ -418,7 +433,7 @@
         scale = lax.rsqrt(jnp.sum(total, axis=1, keepdims=True) / width + NORM_EPS)
         for j in range(2):
             cols = slice(128 * j, 128 * (j + 1))
-            lat[sp, :, cols] = (tiles[j] * scale * kvg[:, cols]).astype(BF16)
+            lat[sp, j * tt : (j + 1) * tt, :] = (tiles[j] * scale * kvg[:, cols]).astype(BF16)
 
     def queries():
         lane = lanes_of((toks, 128))
@@ -434,50 +449,56 @@
             cols = slice(128 * j, 128 * (j + 1))
             qn[:, cols] = (tile * scale * qg[:, cols]).astype(BF16)
 
-    def project(w, cols, at):
-        per = spn // tpn
+    def project(blocks, at):
+        spans = spn // tpn
         acc = None
         for i in range(tpn):
-            block = w[i * per : (i + 1) * per, :, cols].reshape(feat, 256)
+            block = [w[i * spans : (i + 1) * spans, :, n : n + m].reshape(feat, m) for w, n, m in blocks]
+            block = block[0] if len(block) == 1 else jnp.concatenate(block, axis=1)
             part = dot(hall[i], block)
             acc = part if acc is None else acc + part
         left[:, at : at + 256] = acc.astype(BF16)
 
     jobs = {
         1: [line_h.forward],
-        2: [lora, line_k.forward],
-        3: [line_r.forward, latents, plane_l.start, line_q.start],
-        4: [queries],
+        2: [lora],
+        3: [line_k.forward, line_r.forward],
+        4: [latents, plane_l.start, queries],
     }
-    lsteps = list(range(1, plane_l.steps + 1))
     for t in range(1, max(plane_a.steps, 4) + 1):
         if t <= plane_a.steps:
             wstep(t)
         for job in jobs.get(t, []):
             job()
-    if lsteps:
-        plane_l.step(lsteps.pop(0))
-    plane_b.finish()
-    tail = [
-        lambda: (project(wb, slice(0, 256), 256), project(wb, slice(256, 512), 512)),
-        lambda: project(wa, slice(0, 256), 0),
-        scan.prepare,
-        scan.local,
-        line_q.forward,
-    ]
-    while lsteps or tail:
-        if tail:
-            tail.pop(0)()
-        if lsteps:
-            plane_l.step(lsteps.pop(0))
+    plane_b.finish(0, plane_b.steps)
+    project([(wa, 0, 128), (wb, 0, 128)], 256)
+    project([(wb, 128, 256)], 512)
+    scan.prepare()
+    scan.states()
+    steps = plane_l.steps
+
+    def lstep(t):
+        if t <= steps:
+            plane_l.step(t)
+
+    def cstep(t):
+        if t <= steps:
+            plane_c.step(t)
+
+    lstep(1)
+    line_q.forward()
+    lstep(2)
+    plane_c.start()
     scan.join_y()
     line_k.finish()
     line_q.finish()
-    plane_l.finish()
 
     per = CHUNK // tt
+    deep = per // NY
+    chunks = spn // per
     base2 = math.log2(math.e) / math.sqrt(NOPE + ROPE)
-    whole = sp // per
+    own_chunk = sp // per
+    z = sp // NY
 
     def sent(p):
         dev = {"tp": p}
@@ -486,53 +507,87 @@
             remote(sbuf.at[p], srecv.at[tp], s_s.at[p], s_r.at[tp], dev),
         )
 
-    def pair(i, _):
-        p = lax.rem(tp + 1 + i, tpn)
+    def turn(p, _):
         q = dotg(qw[p], qn[...], NT)
         for h in range(2):
             c = slice(h * toks, (h + 1) * toks)
-            qblk[64 * h : 64 * (h + 1), c] = q[64 * h : 64 * (h + 1)].astype(BF16)
+            qblk[p, 64 * h : 64 * (h + 1), c] = q[64 * h : 64 * (h + 1)].astype(BF16)
             a, b = q[128 + 32 * h : 144 + 32 * h], q[144 + 32 * h : 160 + 32 * h]
-            qblk[128:144, c] = (a * qcos[...] - b * qsin[...]).astype(BF16)
-            qblk[144:160, c] = (a * qsin[...] + b * qcos[...]).astype(BF16)
-        msc[...] = jnp.full(msc.shape, NEG_BIG, F32)
-        acc[...] = jnp.zeros(acc.shape, F32)
-
-        def chunk(j, masked):
-            part = lat[pl.ds(j * per, per)].reshape(CHUNK, 384)
-            kv = dot(part[:, : kvw.shape[1]], kvw[p])
-            keys = jnp.concatenate([kv[:, :128].astype(BF16), part[:, 256:]], axis=1)
-            vals = jnp.transpose(kv[:, 128:]).astype(BF16)
-            vals = jnp.concatenate([vals, jnp.ones((16, CHUNK), BF16)], axis=0)
-            for h in range(2):
-                c = slice(h * toks, (h + 1) * toks)
-                s = dot(keys, qblk[:, c])
-                if masked:
-                    at = lax.broadcasted_iota(jnp.int32, (CHUNK, toks), 0)
-                    kpos = (j * per + at // tt) * toks + tp * tt + lax.rem(at, tt)
-                    ok = kpos <= sp * toks + lanes_of((CHUNK, toks))
-                    s = jnp.where(ok, s, NEG_BIG)
-                old = msc[0:1, c]
+            qblk[p, 128:144, c] = (a * qcos[...] - b * qsin[...]).astype(BF16)
+            qblk[p, 144:160, c] = (a * qsin[...] + b * qcos[...]).astype(BF16)
+        return 0
+
+    quart = tt // 4
+
+    def unpack(j):
+        rows = lat[pl.ds(j * per, per), 2 * tt : 2 * tt + quart, :].astype(F32)
+        lane = lanes_of(rows.shape)
+        parts = [
+            jnp.where(lane < 32, pltpu.roll(rows, 128 - 32 * g, 2) if g else rows, 0.0)
+            for g in range(4)
+        ]
+        whole = jnp.stack(parts, axis=1).reshape(CHUNK, 128)
+        krope[pl.ds(pl.multiple_of(j * CHUNK, CHUNK), CHUNK), :] = whole.astype(BF16)
+
+    def chunk(p, j, opening):
+        tiles = kvw.shape[1] // 128
+        part = [lat[pl.ds(j * per, per), i * tt : (i + 1) * tt, :].reshape(CHUNK, 128) for i in range(tiles)]
+        part = part[0] if tiles == 1 else jnp.concatenate(part, axis=1)
+        kv = dot(part, kvw[p])
+        turned = krope[pl.ds(pl.multiple_of(j * CHUNK, CHUNK), CHUNK), :]
+        keys = jnp.concatenate([kv[:, :128].astype(BF16), turned], axis=1)
+        vals = jnp.transpose(kv[:, 128:]).astype(BF16)
+        vals = jnp.concatenate([vals, jnp.ones((16, CHUNK), BF16)], axis=0)
+        for h in range(2):
+            c = slice(h * toks, (h + 1) * toks)
+            s = dot(keys, qblk[p, :, c])
+            if opening:
+                at = lax.broadcasted_iota(jnp.int32, (CHUNK, toks), 0)
+                kpos = (j * per + at // tt) * toks + tp * tt + lax.rem(at, tt)
+                ok = kpos <= sp * toks + lanes_of((CHUNK, toks))
+                s = jnp.where(ok, s, NEG_BIG)
+                new = jnp.max(s, axis=0, keepdims=True)
+                w = jnp.where(ok, jnp.exp2((s - new) * base2), 0.0)
+                acc[p, :, c] = dot(vals, w.astype(BF16))
+            else:
+                old = msc[p, 0:1, c]
                 new = jnp.maximum(old, jnp.max(s, axis=0, keepdims=True))
                 w = jnp.exp2((s - new) * base2)
-                if masked:
-                    w = jnp.where(ok, w, 0.0)
                 fade = jnp.exp2((old - new) * base2)
-                acc[:, c] = acc[:, c] * fade + dot(vals, w.astype(BF16))
-                msc[0:1, c] = new
-
-        @pl.loop(0, whole)
+                acc[p, :, c] = acc[p, :, c] * fade + dot(vals, w.astype(BF16))
+            msc[p, 0:1, c] = new
+
+    def reach(j):
+        far = None
+        for i in range(deep):
+            d = z - (j * deep + i)
+            d = jnp.where(d <= nz // 2, d, nz - d)
+            far = d if far is None else jnp.maximum(far, d)
+        return far
+
+    def each(lo, hi, todo):
+        @pl.loop(0, chunks)
         def _(j):
-            chunk(j, False)
-
-        chunk(whole, True)
+            far = reach(j)
+
+            @pl.when((j < own_chunk) & (far > lo) & (far <= hi))
+            def _():
+                todo(j)
+
+    def opened(p, _):
+        chunk(p, own_chunk, True)
+        return 0
+
+    def close(i, _):
+        p = lax.rem(tp + 1 + i, tpn)
+        each(middle, nz, lambda j: chunk(p, j, False))
         for h in range(2):
             c = slice(h * toks, (h + 1) * toks)
-            total = acc[128:129, c]
+            total = acc[p, 128:129, c]
             some = total > 0.0
             safe = jnp.where(some, total, 1.0)
-            obuf[p, 64 * h : 64 * (h + 1), :] = (acc[64 * h : 64 * (h + 1), c] / safe).astype(BF16)
-            sbuf[p, h : h + 1, :] = jnp.where(some, msc[0:1, c] * base2 + jnp.log2(safe), NEG_BIG)
+            obuf[p, 64 * h : 64 * (h + 1), :] = (acc[p, 64 * h : 64 * (h + 1), c] / safe).astype(BF16)
+            sbuf[p, h : h + 1, :] = jnp.where(some, msc[p, 0:1, c] * base2 + jnp.log2(safe), NEG_BIG)
 
         @pl.when(i < tpn - 1)
         def _():
@@ -541,11 +596,41 @@
 
         return 0
 
-    lax.fori_loop(0, tpn - 2, pair, 0)
+    def early(j):
+        unpack(j)
+
+        @pl.loop(0, tpn)
+        def _(p):
+            chunk(p, j, False)
+
+    lax.fori_loop(0, tpn, turn, 0)
+    half = tpn // 2
+    first, second = min(2, steps), min(3, steps)
+    middle = 2 * second if second > first else 0
+    plane_l.finish(0, first)
+    unpack(own_chunk)
+    lax.fori_loop(0, half, opened, 0)
+    lstep(3)
+    plane_c.begin()
+    lax.fori_loop(half, tpn, opened, 0)
+    lstep(4)
+    cstep(1)
+    plane_l.finish(first + 1, second)
+    if middle:
+        each(0, middle, early)
+    cstep(2)
+    plane_l.finish(second + 1, steps)
+    each(middle, nz, unpack)
+    lax.fori_loop(0, half - 1, close, 0)
+    cstep(3)
+    lax.fori_loop(half - 1, half + 1, close, 0)
+    cstep(4)
     scan.join_z()
-    lax.fori_loop(tpn - 2, tpn, pair, 0)
+    lax.fori_loop(half + 1, tpn, close, 0)
     orecv[tp] = obuf[tp]
     srecv[tp] = sbuf[tp]
+    project([(wc, 0, 256)], 0)
+    scan.inside()
 
     scan.finish()
     cols = []
@@ -619,7 +704,7 @@
     for d in range(1, tpn):
         for c in sent(lax.rem(tp + d, tpn)):
             c.wait_send()
-    for part in (line_h, line_k, line_q, line_r, plane_a, plane_b, plane_l, scan):
+    for part in (line_h, line_k, line_q, line_r, plane_a, plane_b, plane_c, plane_l, scan):
         part.drain()
 
 
@@ -654,14 +739,15 @@
     far = max(nx - 1, 1)
     scratch = [
         VM((tpn, toks, feat), BF16),
+        VM((spn, rw, 128), BF16),
+        VM((spn, rw, 384), BF16),
         VM((spn, rw, 256), BF16),
-        VM((spn, rw, 512), BF16),
         VM((tpn, toks, 128), BF16),
         VM((toks, 128), F32),
         VM((128, tpn * feat), BF16),
         VM((toks, 768), BF16),
         VM((toks, qrank), BF16),
-        VM((spn, tt, 384), BF16),
+        VM((spn, 2 * tt + tt // 4, 128), BF16),
         VM((tpn, kvrank, 256), BF16),
         VM((tpn, 192, qrank), BF16),
         VM(w_out_rec.shape, BF16),
@@ -680,9 +766,10 @@
         VM((nz, 2, vs, HEAD), BF16),
         VM((nz, 8, HEAD), F32),
         VM((NY, 2, vs, HEAD), BF16),
-        VM((256, 2 * toks), BF16),
-        VM((8, 2 * toks), F32),
-        VM((144, 2 * toks), F32),
+        VM((spn * tt, 128), BF16),
+        VM((tpn, 256, 2 * toks), BF16),
+        VM((tpn, 8, 2 * toks), F32),
+        VM((tpn, 144, 2 * toks), F32),
         VM((tpn, 128, toks), BF16),
         VM((tpn, 8, toks), F32),
         VM((tpn, 128, toks), BF16),
@@ -692,11 +779,12 @@
         VM((SPLIT, nx, tt, step), BF16),
         VM((SPLIT, far, tt, step), BF16),
         VM((SPLIT, far, tt, step), BF16),
-        DMA((8,)),
+        DMA((9,)),
         *line, *line, *line, *line,
         DMA(()), DMA((nz - 1, NY)), DMA((NY - 1,)),
-        DMA(()), DMA((nz - 1,)), DMA(()),
-        DMA(()), DMA((nz - 1,)), DMA(()),
+        DMA(()), DMA((nz - 1,)), DMA((nz // 4 + 1,)),
+        DMA(()), DMA((nz - 1, NY)), DMA((NY - 1,)),
+        DMA(()), DMA((nz - 1,)), DMA((nz // 4 + 1,)),
         *([DMA((NY - 1,))] * 4),
         DMA((nz - 1,)), DMA((nz,)), DMA((nz - 1,)), DMA((nz,)),
         *([DMA((NY - 1,))] * 2),

time: 103 us -> 113 us (1.097)
  the two profiles are of different devices: /device:TPU:385 before, /device:TPU:1 now
where the time goes in v3:
time: 113 us
  Pallas kernels  110 us (97%)
  local copies, waits for them, and re-layouts  1.65 us (1%)
  other arithmetic  1.54 us (1%)
    pallas_call x1, Pallas kernels, shards(): pl.pallas_call(functools.partial(mixer_kernel, nz, nx), out_shape=jax.Sha...  110 us

profile of v3, /device:TPU:1, one launch (start us, length us, event | category | flops | bytes accessed | tf_op | source)
XLA Modules:
  0.0 113.3 jit_solution(14650209025732081339)
XLA Ops:
  0.0 0.1 mul.47
  0.1 0.8 fusion
  0.9 0.8 multiply_sine_fusion
  1.6 110.1 %mixer.1 = bf16[32,2048]{1,0:T(8,128)(2,1)} custom-call(bf16[256,256]{1,0:T(8,128)(2,1)} %hid.1, bf16[32,256]{1,0:T(8,128)(2,1)} %wq.1, bf16[32,256]{1,0:T(8,128)(2,1)} %wf.1, bf16[32,256]{1,0:T(8,128)(2,1)} %wi.1, bf16[64,2048]{1,0:T(8,128)(2,1)} %bitcast.9, bf16[32,2048]{1,0:T(8,128)(2,1)} %bitcast.10, bf16[32,2048]{1,0:T(8,128)(2,1)} %bitcast.11, ...), custom_call_target="tpu_custom_call" | custom-call | tf_op jit(solution)/shard_map/mixer/pallas_call | solution.py:801
  111.8 1.6 %copy.20 = bf16[32,2048]{1,0:T(8,128)(2,1)} copy(bf16[32,2048]{1,0:T(8,128)(2,1)} %mixer.1) | data formatting | bytes 262144
  (5 shorter events, 0.0 us)

commit v4 on v3

--- a/solution.py
+++ b/solution.py
@@ -57,6 +57,9 @@
         self.tp, self.core, self.x = tp, lax.rem(tp, 2), tp // 2
         self.sib = self.x * 2 + 1 - self.core
 
+    def near(self):
+        return [1, -1] if self.nx > 2 else [1]
+
     def at_x(self, dx):
         return lax.rem(self.x + dx + self.nx, self.nx) * 2 + self.core
 
@@ -64,21 +67,37 @@
         piece = self.ref.at[slot]
         return remote(piece, piece, self.ssem, self.rsem.at[k], {"tp": to})
 
+    def relay(self, slot, to, k):
+        rows = self.ref.shape[1] // 2
+        piece = self.ref.at[slot, pl.ds(k * rows, rows)]
+        return remote(piece, piece, self.ssem, self.rsem.at[2 + k], {"tp": to})
+
+    def over(self, dx):
+        self.copy(self.at_x(-dx), self.sib, self.nx + dx % self.nx).start()
+
     def start(self):
-        for d in range(1, self.nx):
-            self.copy(self.tp, self.at_x(d), d - 1).start()
-        self.copy(self.tp, self.sib, self.nx - 1).start()
+        for k, d in enumerate(self.near()):
+            self.copy(self.tp, self.at_x(d), k).start()
+        self.over(0)
 
     def forward(self):
-        for d in range(1, self.nx):
+        for k, d in enumerate(self.near()):
             slot = self.at_x(-d)
-            self.copy(slot, self.tp, d - 1).wait_recv()
-            self.copy(slot, self.sib, self.nx - 1 + d).start()
+            self.copy(slot, self.tp, k).wait_recv()
+            if self.nx > 2:
+                self.relay(slot, self.at_x(d), k).start()
+            self.over(d)
+
+    def forward_far(self):
+        if self.nx > 2:
+            for k in range(2):
+                self.relay(self.at_x(2), self.tp, k).wait_recv()
+            self.over(2)
 
     def finish(self):
         for d in range(self.nx):
             x = lax.rem(self.x - d + self.nx, self.nx)
-            self.copy(x * 2 + 1 - self.core, self.tp, self.nx - 1 + d).wait_recv()
+            self.copy(x * 2 + 1 - self.core, self.tp, self.nx + d).wait_recv()
 
     def drain(self):
         take_bytes(self.ref, 2 * self.nx - 1, self.ssem)
@@ -118,26 +137,39 @@
         for c in self.next_of(way, d):
             self.copy(self.slot(-way * d, 0), self.slot(way * (c - d), 0), self.zsem.at[self.key(way, c)]).start()
 
-    def spread(self, slot, t):
-        for d in range(1, NY):
-            self.copy(slot, self.slot(0, d), self.ysem.at[t]).start()
+    def spread(self, slot, t, way):
+        if NY == 2:
+            self.copy(slot, self.slot(0, 1), self.ysem.at[t, 2]).start()
+            return
+        self.copy(slot, self.slot(0, 1), self.ysem.at[t, 0 if way == 1 else 2]).start()
+        self.copy(slot, self.slot(0, -1), self.ysem.at[t, 2 if way == 1 else 1]).start()
 
     def start(self):
         self.hand_on(1, 0)
         self.hand_on(-1, 0)
-        self.spread(self.sp, 0)
+        self.spread(self.sp, 0, 1)
 
     def step(self, t):
         for way, d in self.arrivals(t):
             slot = self.slot(-way * d, 0)
             self.copy(slot, self.sp, self.zsem.at[self.key(way, d)]).wait_recv()
             self.hand_on(way, d)
-            self.spread(slot, t)
+            self.spread(slot, t, way)
+
+    def relay(self, t):
+        if NY == 2 or t > self.steps:
+            return
+        for way in (1, -1):
+            found = [d for w, d in (self.arrivals(t) if t else [(1, 0)]) if w == way]
+            if found:
+                take_bytes(self.ref, len(found), self.ysem.at[t, 0 if way == 1 else 1])
+            for d in found:
+                self.copy(self.slot(-way * d, -way), self.slot(0, way), self.ysem.at[t, 2]).start()
 
     def finish(self, first, last):
         for t in range(first, last + 1):
             count = len(self.arrivals(t)) if t else 1
-            take_bytes(self.ref, count * (NY - 1), self.ysem.at[t])
+            take_bytes(self.ref, count * (1 if NY == 2 else 2), self.ysem.at[t, 2])
 
 
 class PlaneYZ(Plane):
@@ -461,15 +493,18 @@
 
     jobs = {
         1: [line_h.forward],
-        2: [lora],
+        2: [line_h.forward_far, lora],
         3: [line_k.forward, line_r.forward],
-        4: [latents, plane_l.start, queries],
+        4: [line_k.forward_far, line_r.forward_far, latents, plane_l.start, queries],
     }
     for t in range(1, max(plane_a.steps, 4) + 1):
         if t <= plane_a.steps:
             wstep(t)
+        plane_b.relay(t - 1)
         for job in jobs.get(t, []):
             job()
+    for t in range(max(plane_a.steps, 4), plane_b.steps + 1):
+        plane_b.relay(t)
     plane_b.finish(0, plane_b.steps)
     project([(wa, 0, 128), (wb, 0, 128)], 256)
     project([(wb, 128, 256)], 512)
@@ -486,10 +521,17 @@
             plane_c.step(t)
 
     lstep(1)
+    plane_l.relay(0)
+    plane_c.start()
     line_q.forward()
     lstep(2)
-    plane_c.start()
+    plane_l.relay(1)
+    plane_c.begin()
     scan.join_y()
+    line_q.forward_far()
+    lstep(3)
+    plane_l.relay(2)
+    cstep(1)
     line_k.finish()
     line_q.finish()
 
@@ -610,21 +652,19 @@
     plane_l.finish(0, first)
     unpack(own_chunk)
     lax.fori_loop(0, half, opened, 0)
-    lstep(3)
-    plane_c.begin()
+    lstep(4)
+    plane_l.relay(3)
+    cstep(2)
     lax.fori_loop(half, tpn, opened, 0)
-    lstep(4)
-    cstep(1)
+    plane_l.relay(4)
+    cstep(3)
     plane_l.finish(first + 1, second)
     if middle:
         each(0, middle, early)
-    cstep(2)
+    cstep(4)
     plane_l.finish(second + 1, steps)
     each(middle, nz, unpack)
-    lax.fori_loop(0, half - 1, close, 0)
-    cstep(3)
-    lax.fori_loop(half - 1, half + 1, close, 0)
-    cstep(4)
+    lax.fori_loop(0, half + 1, close, 0)
     scan.join_z()
     lax.fori_loop(half + 1, tpn, close, 0)
     orecv[tp] = obuf[tp]
@@ -682,25 +722,39 @@
         first = pl.multiple_of((2 * i + core) * tt, tt)
         return mixed[pl.ds(first, tt), k * step : (k + 1) * step] + got_pair[k, i].astype(F32)
 
-    def final(d, k):
-        to = lax.rem(x + d, nx) * 2 + core
-        return remote(sums.at[k, d - 1], got.at[k, d - 1], f_s.at[k, d - 1], f_r.at[k, d - 1], {"tp": to})
-
-    for k in range(width // step):
+    def final(k, n):
+        way = 1 if k % 2 == 0 else -1
+        to = lax.rem(x + (-way if n == 1 else way) + nx, nx) * 2 + core
+        return remote(sums.at[k, n], got.at[k, n], f_s.at[k, n], f_r.at[k, n], {"tp": to})
+
+    pieces = range(width // step)
+    kinds = [0, 1, 2] if nx > 2 else [0]
+    for k in pieces:
+        way = 1 if k % 2 == 0 else -1
         to_sib(k).wait_recv()
-        for d in range(1, nx):
-            sums[k, d - 1] = mine(lax.rem(x + d, nx), k).astype(BF16)
-            final(d, k).start()
-    for k in range(width // step):
+        if nx > 2:
+            sums[k, 2] = mine(lax.rem(x + 2, nx), k).astype(BF16)
+            final(k, 2).start()
+            sums[k, 1] = mine(lax.rem(x - way + nx, nx), k).astype(BF16)
+            final(k, 1).start()
+    for k in pieces:
+        way = 1 if k % 2 == 0 else -1
+        passed = mine(lax.rem(x + way + nx, nx), k)
+        if nx > 2:
+            final(k, 2).wait_recv()
+            passed = passed + got[k, 2].astype(F32)
+        sums[k, 0] = passed.astype(BF16)
+        final(k, 0).start()
+    for k in pieces:
         total = mine(x, k)
-        for d in range(1, nx):
-            final(d, k).wait_recv()
-            total = total + got[k, d - 1].astype(F32)
+        for n in kinds[:2]:
+            final(k, n).wait_recv()
+            total = total + got[k, n].astype(F32)
         out[:, k * step : (k + 1) * step] = total.astype(BF16)
-    for k in range(width // step):
+    for k in pieces:
         to_sib(k).wait_send()
-        for d in range(1, nx):
-            final(d, k).wait_send()
+        for n in kinds:
+            final(k, n).wait_send()
     for d in range(1, tpn):
         for c in sent(lax.rem(tp + d, tpn)):
             c.wait_send()
@@ -735,8 +789,8 @@
 
     vs = HEAD // NY
     step = width // SPLIT
-    line = [DMA(()), DMA((2 * nx - 1,))]
-    far = max(nx - 1, 1)
+    line = [DMA(()), DMA((2 * nx,))]
+    far = 3
     scratch = [
         VM((tpn, toks, feat), BF16),
         VM((spn, rw, 128), BF16),
@@ -782,9 +836,9 @@
         DMA((9,)),
         *line, *line, *line, *line,
         DMA(()), DMA((nz - 1, NY)), DMA((NY - 1,)),
-        DMA(()), DMA((nz - 1,)), DMA((nz // 4 + 1,)),
+        DMA(()), DMA((nz - 1,)), DMA((nz // 4 + 1, 3)),
         DMA(()), DMA((nz - 1, NY)), DMA((NY - 1,)),
-        DMA(()), DMA((nz - 1,)), DMA((nz // 4 + 1,)),
+        DMA(()), DMA((nz - 1,)), DMA((nz // 4 + 1, 3)),
         *([DMA((NY - 1,))] * 4),
         DMA((nz - 1,)), DMA((nz,)), DMA((nz - 1,)), DMA((nz,)),
         *([DMA((NY - 1,))] * 2),

time: 113 us -> 112 us (level)
  the two profiles are of different devices: /device:TPU:1 before, /device:TPU:416 now
where the time goes in v4:
time: 112 us
  Pallas kernels  109 us (97%)
  local copies, waits for them, and re-layouts  1.65 us (1%)
  other arithmetic  1.54 us (1%)
    pallas_call x1, Pallas kernels, shards(): pl.pallas_call(functools.partial(mixer_kernel, nz, nx), out_shape=jax.Sha...  109 us

profile of v4, /device:TPU:416, one launch (start us, length us, event | category | flops | bytes accessed | tf_op | source)
XLA Modules:
  0.0 112.1 jit_solution(4442001650224723927)
XLA Ops:
  0.0 0.1 mul.47
  0.1 0.8 fusion
  0.9 0.8 multiply_sine_fusion
  1.6 108.9 %mixer.1 = bf16[32,2048]{1,0:T(8,128)(2,1)} custom-call(bf16[256,256]{1,0:T(8,128)(2,1)} %hid.1, bf16[32,256]{1,0:T(8,128)(2,1)} %wq.1, bf16[32,256]{1,0:T(8,128)(2,1)} %wf.1, bf16[32,256]{1,0:T(8,128)(2,1)} %wi.1, bf16[64,2048]{1,0:T(8,128)(2,1)} %bitcast.9, bf16[32,2048]{1,0:T(8,128)(2,1)} %bitcast.10, bf16[32,2048]{1,0:T(8,128)(2,1)} %bitcast.11, ...), custom_call_target="tpu_custom_call" | custom-call | tf_op jit(solution)/shard_map/mixer/pallas_call | solution.py:855
  110.6 1.6 %copy.20 = bf16[32,2048]{1,0:T(8,128)(2,1)} copy(bf16[32,2048]{1,0:T(8,128)(2,1)} %mixer.1) | data formatting | bytes 262144
  (5 shorter events, 0.0 us)

commit v5 on v3

--- a/solution.py
+++ b/solution.py
@@ -17,7 +17,6 @@
 NY = 4
 CHUNK = 512
 SPLIT = 4
-FULL_GREET = False
 MESH = pl.DeviceIdType.MESH
 F32 = jnp.float32
 BF16 = jnp.bfloat16
@@ -85,12 +84,14 @@
 
 
 class Plane:
+    jump = 2
+
     def __init__(self, ref, ssem, zsem, ysem, nz):
         self.ref, self.ssem, self.zsem, self.ysem, self.nz = ref, ssem, zsem, ysem, nz
         self.sp = lax.axis_index("sp")
         self.z, self.y = self.sp // NY, lax.rem(self.sp, NY)
         self.limit = {1: nz // 2, -1: nz // 2 - 1}
-        self.steps = (nz // 2 + 1) // 2
+        self.steps = -(-(nz // 2) // self.jump)
 
     def slot(self, dz, dy):
         z = lax.rem(self.z + dz + self.nz, self.nz)
@@ -101,19 +102,24 @@
         return remote(piece, piece, self.ssem, sem, {"sp": to})
 
     def next_of(self, way, d):
-        return [c for c in (d + 2, d + 1) if d % 2 == 0 and c <= self.limit[way]]
+        ahead = [d + self.jump] + [d + i for i in range(1, self.jump)]
+        return [c for c in ahead if d % self.jump == 0 and c <= self.limit[way]]
 
     def key(self, way, d):
         return d - 1 if way == 1 else self.limit[1] + d - 1
 
     def arrivals(self, t):
-        return [(w, d) for d in (2 * t - 1, 2 * t) for w in (1, -1) if d <= self.limit[w]]
+        top = self.jump * t
+        order = [top - 1, top] if self.jump == 2 else [top - 3, top - 2, top, top - 1]
+        return [(w, d) for d in order for w in (1, -1) if d <= self.limit[w]]
 
     def drain(self):
         take_bytes(self.ref, self.nz * NY - 1, self.ssem)
 
 
 class PlaneZY(Plane):
+    jump = 4
+
     def hand_on(self, way, d):
         for c in self.next_of(way, d):
             self.copy(self.slot(-way * d, 0), self.slot(way * (c - d), 0), self.zsem.at[self.key(way, c)]).start()
@@ -327,12 +333,12 @@
 def mixer_kernel(
     nz, nx, hid, wq, wf, wi, wqdt, wkvdt, wkrt, wku, wvu, wqn, wqrt, qg, kvg, kcos, ksin, qcos, qsin,
     gap, dext, gain, worh, woah, out,
-    hall, wa, wb, wc, rall, racc, wrt, left, qn, lat, kvw, qw, wor, woa,
+    hall, wa, wb, wc, rall, kvin, racc, wrt, left, qn, lat, kvw, qw, wor, woa,
     lout, qx, into, key, cum, stb, decb, ys, yd, zb, zdb, zs, zd, ib,
     krope, qblk, msc, acc, obuf, sbuf, orecv, srecv, mixed, pairs, got_pair, sums, got,
     loc, hs, hr, ks, kr, qs, qr, rs, rr, was, waz, way_, wbs, wbz, wby, wcs, wcz, wcy, ls, lz, ly,
     ys_s, ys_r, yd_s, yd_r, zs_s, zs_r, zd_s, zd_r, i_s, i_r,
-    o_s, o_r, s_s, s_r, p_s, p_r, f_s, f_r,
+    o_s, o_r, s_s, s_r, kv_s, kv_r, p_s, p_r, f_s, f_r,
 ):
     tpn, spn = 2 * nx, nz * NY
     tp, sp = lax.axis_index("tp"), lax.axis_index("sp")
@@ -343,7 +349,7 @@
     line_q, line_r = Line(qw, qs, qr, nx), Line(rall, rs, rr, nx)
     plane_a = PlaneYZ(wa, was, waz, way_, nz)
     plane_b = PlaneZY(wb, wbs, wbz, wby, nz)
-    plane_c = PlaneYZ(wc, wcs, wcz, wcy, nz)
+    plane_c = PlaneZY(wc, wcs, wcz, wcy, nz)
     plane_l = PlaneZY(lat, ls, lz, ly, nz)
     sems = (ys_s, ys_r, yd_s, yd_r, zs_s, zs_r, zd_s, zd_r, i_s, i_r)
     scan = Scan(nz, left, gap, dext, lout, qx, into, key, cum, stb, decb, ys, yd, zb, zdb, zs, zd, ib, sems)
@@ -351,7 +357,7 @@
     barrier = pltpu.get_barrier_semaphore()
     greet = [{"tp": lax.rem(tp + d, tpn)} for d in range(1, tpn)]
     greet += [{"sp": plane_a.slot(0, d)} for d in range(1, NY)]
-    near = [d for d in range(1, nz) if FULL_GREET or d <= 2 or d >= nz - 2]
+    near = [d for d in range(1, nz) if d <= 4 or d >= nz - 4]
     greet += [{"sp": plane_a.slot(d, 0)} for d in near]
     for dev in greet:
         pl.semaphore_signal(barrier, inc=1, device_id=dev, device_id_type=MESH)
@@ -378,7 +384,6 @@
     line_h.start()
     plane_a.start()
     plane_b.start()
-    line_k.start()
     qw[tp, 0:128, :] = jnp.transpose(wqn[...].astype(F32)).astype(BF16)
     qw[tp, 128:192, :] = wqrt[...]
     qblk[...] = jnp.zeros(qblk.shape, BF16)
@@ -387,6 +392,10 @@
     def wstep(t):
         plane_b.step(t)
         plane_a.step(t)
+
+    def kv_copy(to):
+        mine = rall.at[tp, pl.ds(pl.multiple_of(to * tt, tt), tt)]
+        return remote(mine, kvin.at[tp], kv_s.at[to], kv_r.at[tp], {"tp": to})
 
     def lora():
         line_h.finish()
@@ -395,8 +404,12 @@
             part = dotg(hall[i], wrt[:, i * feat : (i + 1) * feat], NT)
             acc = part if acc is None else acc + part
         rall[tp] = acc.astype(BF16)
+        for d in range(1, tpn):
+            kv_copy(lax.rem(tp + d, tpn)).start()
         line_r.start()
+        line_k.start()
         line_q.start()
+        kvin[tp] = rall[tp, pl.ds(pl.multiple_of(tp * tt, tt), tt), :]
         racc[...] = acc
         mine = racc[pl.ds(pl.multiple_of(tp * tt, tt), tt), :]
         lane = lanes_of((tt, 128))
@@ -414,8 +427,9 @@
         lat[sp, 2 * tt : 2 * tt + quart, :] = packed.astype(BF16)
 
     def latents():
-        line_r.finish()
-        first = pl.multiple_of(tp * tt, tt)
+        for d in range(1, tpn):
+            src = lax.rem(tp + d, tpn)
+            remote(kvin.at[src], kvin.at[src], kv_s.at[src], kv_r.at[src], {"tp": tp}).wait_recv()
         lane = lanes_of((tt, 128))
         tiles = []
         total = jnp.zeros((tt, 128), F32)
@@ -425,7 +439,7 @@
             for k in range(4):
                 if 4 * j + k >= tpn:
                     continue
-                piece = rall[4 * j + k, pl.ds(first, tt), :].astype(F32)
+                piece = kvin[4 * j + k].astype(F32)
                 moved = pltpu.roll(piece, (32 * k - 64) % 128, 1) if k != 2 else piece
                 tile = jnp.where((lane >= 32 * k) & (lane < 32 * (k + 1)), moved, tile)
             tiles.append(tile)
@@ -436,6 +450,7 @@
             lat[sp, j * tt : (j + 1) * tt, :] = (tiles[j] * scale * kvg[:, cols]).astype(BF16)
 
     def queries():
+        line_r.finish()
         lane = lanes_of((toks, 128))
         total = jnp.zeros((toks, 128), F32)
         for i in range(tpn):
@@ -459,37 +474,36 @@
             acc = part if acc is None else acc + part
         left[:, at : at + 256] = acc.astype(BF16)
 
-    jobs = {
-        1: [line_h.forward],
-        2: [lora],
-        3: [line_k.forward, line_r.forward],
-        4: [latents, plane_l.start, queries],
-    }
-    for t in range(1, max(plane_a.steps, 4) + 1):
-        if t <= plane_a.steps:
-            wstep(t)
-        for job in jobs.get(t, []):
-            job()
+    def step(plane, t):
+        if t <= plane.steps:
+            plane.step(t)
+
+    step(plane_a, 1)
+    step(plane_b, 1)
+    line_h.forward()
+    step(plane_a, 2)
+    step(plane_b, 2)
+    lora()
+    step(plane_a, 3)
+    latents()
+    plane_l.start()
+    step(plane_a, 4)
+    plane_c.start()
+    line_r.forward()
     plane_b.finish(0, plane_b.steps)
     project([(wa, 0, 128), (wb, 0, 128)], 256)
     project([(wb, 128, 256)], 512)
     scan.prepare()
     scan.states()
     steps = plane_l.steps
-
-    def lstep(t):
-        if t <= steps:
-            plane_l.step(t)
-
-    def cstep(t):
-        if t <= steps:
-            plane_c.step(t)
-
-    lstep(1)
+    step(plane_l, 1)
+    line_k.forward()
+    step(plane_c, 1)
+    scan.join_y()
+    step(plane_l, 2)
+    queries()
     line_q.forward()
-    lstep(2)
-    plane_c.start()
-    scan.join_y()
+    step(plane_c, 2)
     line_k.finish()
     line_q.finish()
 
@@ -605,30 +619,20 @@
 
     lax.fori_loop(0, tpn, turn, 0)
     half = tpn // 2
-    first, second = min(2, steps), min(3, steps)
-    middle = 2 * second if second > first else 0
-    plane_l.finish(0, first)
+    middle = plane_l.jump if steps > 1 else 0
+    plane_l.finish(0, 1)
     unpack(own_chunk)
-    lax.fori_loop(0, half, opened, 0)
-    lstep(3)
-    plane_c.begin()
-    lax.fori_loop(half, tpn, opened, 0)
-    lstep(4)
-    cstep(1)
-    plane_l.finish(first + 1, second)
+    lax.fori_loop(0, tpn, opened, 0)
     if middle:
         each(0, middle, early)
-    cstep(2)
-    plane_l.finish(second + 1, steps)
+    plane_l.finish(2, steps)
     each(middle, nz, unpack)
-    lax.fori_loop(0, half - 1, close, 0)
-    cstep(3)
-    lax.fori_loop(half - 1, half + 1, close, 0)
-    cstep(4)
+    lax.fori_loop(0, half + 1, close, 0)
     scan.join_z()
     lax.fori_loop(half + 1, tpn, close, 0)
     orecv[tp] = obuf[tp]
     srecv[tp] = sbuf[tp]
+    plane_c.finish(0, plane_c.steps)
     project([(wc, 0, 256)], 0)
     scan.inside()
 
@@ -704,6 +708,7 @@
     for d in range(1, tpn):
         for c in sent(lax.rem(tp + d, tpn)):
             c.wait_send()
+        kv_copy(lax.rem(tp + d, tpn)).wait_send()
     for part in (line_h, line_k, line_q, line_r, plane_a, plane_b, plane_c, plane_l, scan):
         part.drain()
 
@@ -743,6 +748,7 @@
         VM((spn, rw, 384), BF16),
         VM((spn, rw, 256), BF16),
         VM((tpn, toks, 128), BF16),
+        VM((tpn, tt, 128), BF16),
         VM((toks, 128), F32),
         VM((128, tpn * feat), BF16),
         VM((toks, 768), BF16),
@@ -783,12 +789,12 @@
         *line, *line, *line, *line,
         DMA(()), DMA((nz - 1, NY)), DMA((NY - 1,)),
         DMA(()), DMA((nz - 1,)), DMA((nz // 4 + 1,)),
-        DMA(()), DMA((nz - 1, NY)), DMA((NY - 1,)),
+        DMA(()), DMA((nz - 1,)), DMA((nz // 4 + 1,)),
         DMA(()), DMA((nz - 1,)), DMA((nz // 4 + 1,)),
         *([DMA((NY - 1,))] * 4),
         DMA((nz - 1,)), DMA((nz,)), DMA((nz - 1,)), DMA((nz,)),
         *([DMA((NY - 1,))] * 2),
-        *([DMA((tpn,))] * 4),
+        *([DMA((tpn,))] * 6),
         *([DMA((SPLIT,))] * 2),
         *([DMA((SPLIT, far))] * 2),
     ]
@@ -801,7 +807,7 @@
     return pl.pallas_call(
         functools.partial(mixer_kernel, nz, nx),
         out_shape=jax.ShapeDtypeStruct((tt, width), BF16),
-        in_specs=[whole] * (len(args) - 2) + [anywhere] * 2,
+        in_specs=[anywhere if i in (0, 1, 2, 3, 7, 8, 20, 21) else whole for i in range(len(args))],
         out_specs=whole,
         scratch_shapes=scratch,
         compiler_params=pltpu.CompilerParams(

time: 113 us -> 108 us (0.956)
  the two profiles are of different devices: /device:TPU:1 before, /device:TPU:417 now
where the time goes in v5:
time: 108 us
  Pallas kernels  105 us (97%)
  local copies, waits for them, and re-layouts  1.65 us (2%)
  other arithmetic  1.54 us (1%)
    pallas_call x1, Pallas kernels, shards(): pl.pallas_call(functools.partial(mixer_kernel, nz, nx), out_shape=jax.Sha...  105 us

profile of v5, /device:TPU:417, one launch (start us, length us, event | category | flops | bytes accessed | tf_op | source)
XLA Modules:
  0.0 107.8 jit_solution(6739623267678071559)
XLA Ops:
  0.0 0.1 mul.47
  0.1 0.8 fusion
  0.9 0.8 multiply_sine_fusion
  1.6 104.6 %mixer.1 = bf16[32,2048]{1,0:T(8,128)(2,1)} custom-call(bf16[256,256]{1,0:T(8,128)(2,1)} %hid.1, bf16[32,256]{1,0:T(8,128)(2,1)} %wq.1, bf16[32,256]{1,0:T(8,128)(2,1)} %wf.1, bf16[32,256]{1,0:T(8,128)(2,1)} %wi.1, bf16[64,2048]{1,0:T(8,128)(2,1)} %bitcast.9, bf16[32,2048]{1,0:T(8,128)(2,1)} %bitcast.10, bf16[32,2048]{1,0:T(8,128)(2,1)} %bitcast.11, ...), custom_call_target="tpu_custom_call" | custom-call | tf_op jit(solution)/shard_map/mixer/pallas_call | solution.py:807
  106.3 1.6 %copy.20 = bf16[32,2048]{1,0:T(8,128)(2,1)} copy(bf16[32,2048]{1,0:T(8,128)(2,1)} %mixer.1) | data formatting | bytes 262144
  (5 shorter events, 0.0 us)

commit v6 on v2

--- a/solution.py
+++ b/solution.py
@@ -17,7 +17,6 @@
 NY = 4
 CHUNK = 512
 SPLIT = 4
-FULL_GREET = False
 MESH = pl.DeviceIdType.MESH
 F32 = jnp.float32
 BF16 = jnp.bfloat16
@@ -322,12 +321,12 @@
 def mixer_kernel(
     nz, nx, hid, wq, wf, wi, wqdt, wkvdt, wkrt, wku, wvu, wqn, wqrt, qg, kvg, kcos, ksin, qcos, qsin,
     gap, dext, gain, worh, woah, out,
-    hall, wa, wb, rall, racc, wrt, left, qn, lat, kvw, qw, wor, woa,
+    hall, wa, wb, rall, kvin, racc, wrt, left, qn, lat, kvw, qw, wor, woa,
     lout, qx, into, key, cum, stb, decb, ys, yd, zb, zdb, zs, zd, ib,
     qblk, msc, acc, obuf, sbuf, orecv, srecv, mixed, pairs, got_pair, sums, got,
     loc, hs, hr, ks, kr, qs, qr, rs, rr, was, waz, way_, wbs, wbz, wby, ls, lz, ly,
     ys_s, ys_r, yd_s, yd_r, zs_s, zs_r, zd_s, zd_r, i_s, i_r,
-    o_s, o_r, s_s, s_r, p_s, p_r, f_s, f_r,
+    o_s, o_r, s_s, s_r, kv_s, kv_r, p_s, p_r, f_s, f_r,
 ):
     tpn, spn = 2 * nx, nz * NY
     tp, sp = lax.axis_index("tp"), lax.axis_index("sp")
@@ -345,7 +344,7 @@
     barrier = pltpu.get_barrier_semaphore()
     greet = [{"tp": lax.rem(tp + d, tpn)} for d in range(1, tpn)]
     greet += [{"sp": plane_a.slot(0, d)} for d in range(1, NY)]
-    near = [d for d in range(1, nz) if FULL_GREET or d <= 2 or d >= nz - 2]
+    near = [d for d in range(1, nz) if d <= 2 or d >= nz - 2]
     greet += [{"sp": plane_a.slot(d, 0)} for d in near]
     for dev in greet:
         pl.semaphore_signal(barrier, inc=1, device_id=dev, device_id_type=MESH)
@@ -371,7 +370,6 @@
     line_h.start()
     plane_a.start()
     plane_b.start()
-    line_k.start()
     qw[tp, 0:128, :] = jnp.transpose(wqn[...].astype(F32)).astype(BF16)
     qw[tp, 128:192, :] = wqrt[...]
     qblk[...] = jnp.zeros(qblk.shape, BF16)
@@ -380,6 +378,10 @@
     def wstep(t):
         plane_b.step(t)
         plane_a.step(t)
+
+    def kv_copy(to):
+        mine = rall.at[tp, pl.ds(pl.multiple_of(to * tt, tt), tt)]
+        return remote(mine, kvin.at[tp], kv_s.at[to], kv_r.at[tp], {"tp": to})
 
     def lora():
         line_h.finish()
@@ -388,7 +390,12 @@
             part = dotg(hall[i], wrt[:, i * feat : (i + 1) * feat], NT)
             acc = part if acc is None else acc + part
         rall[tp] = acc.astype(BF16)
+        for d in range(1, tpn):
+            kv_copy(lax.rem(tp + d, tpn)).start()
         line_r.start()
+        line_k.start()
+        line_q.start()
+        kvin[tp] = rall[tp, pl.ds(pl.multiple_of(tp * tt, tt), tt), :]
         racc[...] = acc
         mine = racc[pl.ds(pl.multiple_of(tp * tt, tt), tt), :]
         lane = lanes_of((tt, 128))
@@ -399,8 +406,9 @@
         lat[sp, :, 256:384] = jnp.where(lane < 32, pltpu.roll(turned, 32, 1), 0.0).astype(BF16)
 
     def latents():
-        line_r.finish()
-        first = pl.multiple_of(tp * tt, tt)
+        for d in range(1, tpn):
+            src = lax.rem(tp + d, tpn)
+            remote(kvin.at[src], kvin.at[src], kv_s.at[src], kv_r.at[src], {"tp": tp}).wait_recv()
         lane = lanes_of((tt, 128))
         tiles = []
         total = jnp.zeros((tt, 128), F32)
@@ -410,7 +418,7 @@
             for k in range(4):
                 if 4 * j + k >= tpn:
                     continue
-                piece = rall[4 * j + k, pl.ds(first, tt), :].astype(F32)
+                piece = kvin[4 * j + k].astype(F32)
                 moved = pltpu.roll(piece, (32 * k - 64) % 128, 1) if k != 2 else piece
                 tile = jnp.where((lane >= 32 * k) & (lane < 32 * (k + 1)), moved, tile)
             tiles.append(tile)
@@ -421,6 +429,7 @@
             lat[sp, :, cols] = (tiles[j] * scale * kvg[:, cols]).astype(BF16)
 
     def queries():
+        line_r.finish()
         lane = lanes_of((toks, 128))
         total = jnp.zeros((toks, 128), F32)
         for i in range(tpn):
@@ -445,9 +454,9 @@
 
     jobs = {
         1: [line_h.forward],
-        2: [lora, line_k.forward],
-        3: [line_r.forward, latents, plane_l.start, line_q.start],
-        4: [queries],
+        2: [lora],
+        3: [latents, plane_l.start, line_r.forward],
+        4: [line_k.forward, queries],
     }
     lsteps = list(range(1, plane_l.steps + 1))
     for t in range(1, max(plane_a.steps, 4) + 1):
@@ -619,6 +628,7 @@
     for d in range(1, tpn):
         for c in sent(lax.rem(tp + d, tpn)):
             c.wait_send()
+        kv_copy(lax.rem(tp + d, tpn)).wait_send()
     for part in (line_h, line_k, line_q, line_r, plane_a, plane_b, plane_l, scan):
         part.drain()
 
@@ -657,6 +667,7 @@
         VM((spn, rw, 256), BF16),
         VM((spn, rw, 512), BF16),
         VM((tpn, toks, 128), BF16),
+        VM((tpn, tt, 128), BF16),
         VM((toks, 128), F32),
         VM((128, tpn * feat), BF16),
         VM((toks, 768), BF16),
@@ -700,7 +711,7 @@
         *([DMA((NY - 1,))] * 4),
         DMA((nz - 1,)), DMA((nz,)), DMA((nz - 1,)), DMA((nz,)),
         *([DMA((NY - 1,))] * 2),
-        *([DMA((tpn,))] * 4),
+        *([DMA((tpn,))] * 6),
         *([DMA((SPLIT,))] * 2),
         *([DMA((SPLIT, far))] * 2),
     ]
@@ -713,7 +724,7 @@
     return pl.pallas_call(
         functools.partial(mixer_kernel, nz, nx),
         out_shape=jax.ShapeDtypeStruct((tt, width), BF16),
-        in_specs=[whole] * (len(args) - 2) + [anywhere] * 2,
+        in_specs=[anywhere if i in (0, 1, 2, 3, 7, 8, 20, 21) else whole for i in range(len(args))],
         out_specs=whole,
         scratch_shapes=scratch,
         compiler_params=pltpu.CompilerParams(

time: 103 us -> 102 us (level)
  Pallas kernels: 99.9 us -> 98.5 us
    pallas_call x1, Pallas kernels: 99.9 us -> 98.5 us  [shards(): pl.pallas_call(functools.partial(mixer_kernel, nz, nx), out_shape=jax.Sha...]
where the time goes in v6:
time: 102 us
  Pallas kernels  98.5 us (97%)
  local copies, waits for them, and re-layouts  1.65 us (2%)
  other arithmetic  1.54 us (2%)
    pallas_call x1, Pallas kernels, shards(): pl.pallas_call(functools.partial(mixer_kernel, nz, nx), out_shape=jax.Sha...  98.5 us

profile of v6, /device:TPU:385, one launch (start us, length us, event | category | flops | bytes accessed | tf_op | source)
XLA Modules:
  0.0 101.8 jit_solution(7391446275122721765)
XLA Ops:
  0.0 0.1 mul.47
  0.1 0.8 fusion
  0.9 0.8 multiply_sine_fusion
  1.6 98.5 %mixer.1 = bf16[32,2048]{1,0:T(8,128)(2,1)} custom-call(bf16[256,256]{1,0:T(8,128)(2,1)} %hid.1, bf16[32,256]{1,0:T(8,128)(2,1)} %wq.1, bf16[32,256]{1,0:T(8,128)(2,1)} %wf.1, bf16[32,256]{1,0:T(8,128)(2,1)} %wi.1, bf16[64,2048]{1,0:T(8,128)(2,1)} %bitcast.9, bf16[32,2048]{1,0:T(8,128)(2,1)} %bitcast.10, bf16[32,2048]{1,0:T(8,128)(2,1)} %bitcast.11, ...), custom_call_target="tpu_custom_call" | custom-call | tf_op jit(solution)/shard_map/mixer/pallas_call | solution.py:724
  100.2 1.6 %copy.20 = bf16[32,2048]{1,0:T(8,128)(2,1)} copy(bf16[32,2048]{1,0:T(8,128)(2,1)} %mixer.1) | data formatting | bytes 262144
  (5 shorter events, 0.0 us)
